TPU v7x, 512 devices: a whole 4x8x8 slice. The times are simulated.
512 devices in a mesh: sp: 64 (over z, y), tp: 8 (over x, core).
Axes of the slice: x: 4, y: 8, z: 8, core: 2. Of those that a mesh axis runs over, the one named last changes fastest.
Arguments:
- lookup_request_vectors: bfloat16 [16384, 1024], P('sp', 'tp'), may hold values from -6 to 6
- lookup_address_vectors: bfloat16 [16384, 1024], P('sp', 'tp'), may hold values from -6 to 6
- lookup_content_vectors: bfloat16 [16384, 1024], P('sp', 'tp'), may hold values from -6 to 6
- admission_preactivation: float32 [2, 16, 16384], P(None, 'tp', 'sp'), may hold values from -3 to 250
- retention_preactivation: float32 [2, 16, 16384], P(None, 'tp', 'sp'), may hold values from 0 to 20
- extra_decay_terms: float32 [2, 16, 16384], P(None, 'tp', 'sp'), may hold values from -0.6 to 0
- per_slot_rescale_factor: float32 [1024], P('tp'), may hold values from 0.1 to 1.9
- mixer_exit_matrix: bfloat16 [1024, 2048], P('tp'), may hold values from -0.1875 to 0.1875
- skip_path_activity: bfloat16 [16384, 2048], P(('sp', 'tp')), may hold values from -6 to 6
- mlp_rescale_factor: float32 [2048], replicated, may hold values from 0.1 to 1.9
- filter_widening_matrix: bfloat16 [2048, 5632], P('sp', 'tp'), may hold values from -0.125 to 0.125
- multiplier_widening_matrix: bfloat16 [2048, 5632], P('sp', 'tp'), may hold values from -0.125 to 0.125
- neighbour_filter_coefficients: float32 [3, 5632], P(None, 'tp'), may hold values from -3.5 to 3.5
- contracting_matrix: bfloat16 [5632, 2048], P('tp', 'sp'), may hold values from -0.078125 to 0.078125
Outputs:
- result: bfloat16 [16384, 2048], P(('sp', 'tp'))
All inputs are finite; a program needn't handle non-finite values.
Results may differ from a plain program's by a relative error of at most 0.018.
Values may be sent and summed in bfloat16 or wider, within the bound.
No kernel may reach another device: no remote copies, remote signals or barrier semaphores. Data moves between devices by JAX's collectives and lax.ppermute only.
A program may use at most 64 MiB of HBM per device.

v0:
```python
import jax
import jax.numpy as jnp
from jax import lax
from jax.sharding import Mesh
from jax.sharding import PartitionSpec as P

HEAD_DIM = 64
BLOCK = 128
SP = ("sp_0", "sp_1")
SP_TP = ("sp_0", "sp_1", "tp")


precise_mode = lax.Precision.HIGHEST
epsilon = 1e-06
far_below = -1e30


def nothing_yet(shard, identity):
    return jax.tree.map(
        lambda a, e: jnp.broadcast_to(jnp.asarray(e, a.dtype), a.shape), shard, identity
    )


def gathered_once(shard, axis):
    leaves = jax.tree.leaves(shard)
    order = sorted(range(len(leaves)), key=lambda k: -leaves[k].size)
    width = (1, *leaves[order[0]].shape)[-1]
    lines = [
        jnp.pad(leaves[k].reshape(-1), (0, -leaves[k].size % width)).reshape(-1, width)
        for k in order
    ]
    both, at, found = (lax.all_gather(jnp.concatenate(lines), axis), 0, {})
    for k, line in zip(order, lines):
        section = both[:, at : at + len(line)].reshape(len(both), -1)
        found[k] = section[:, : leaves[k].size].reshape(-1, *leaves[k].shape)
        at += len(line)
    numbers = iter(range(len(leaves)))
    return jax.tree.map(lambda _: found[next(numbers)], shard)


def prefix_by_axis(shard, axes, combine, identity, reverse):
    before = start = nothing_yet(shard, identity)
    running = shard
    for axis in reversed(axes):
        peers, here = (lax.axis_size(axis), lax.axis_index(axis))
        pieces = gathered_once(running, axis)
        inside, running = (start, start)
        for k in reversed(range(peers)) if reverse else range(peers):
            passed = k > here if reverse else k < here
            running = combine(running, jax.tree.map(lambda part: part[k], pieces))
            inside = jax.tree.map(lambda new, old: jnp.where(passed, new, old), running, inside)
        before = combine(inside, before)
    return before


def from_everyone(shard, axis):
    copies = jnp.broadcast_to(shard, (lax.axis_size(axis), *shard.shape))
    return lax.all_to_all(copies, axis, split_axis=0, concat_axis=0, tiled=True)


def laid_out(pieces, dim):
    dims = list(pieces.shape[1:])
    dims[dim] *= pieces.shape[0]
    return jnp.moveaxis(pieces, 0, dim).reshape(dims)


def collect(shard, axis, dim):
    pieces = from_everyone(shard, axis)
    return laid_out(pieces, dim)


def side_by_side(arrays, axis, dim, along):
    ends, at = ([], 0)
    for a in arrays[:-1]:
        at += a.shape[along]
        ends.append(at)
    both = jnp.concatenate(arrays, axis=along)
    return tuple(jnp.split(lax.all_gather(both, axis, axis=dim, tiled=True), ends, axis=along))


def extended(shard, sides, width):
    for axis, dim in sides:
        peers, length = (lax.axis_size(axis), shard.shape[dim])
        up = [(i, (i + 1) % peers) for i in range(peers - 1)]
        down = [(j, i) for i, j in up]
        last = lax.slice_in_dim(shard, length - width, length, axis=dim)
        first = lax.slice_in_dim(shard, 0, width, axis=dim)
        before = lax.ppermute(last, axis, up)
        after = lax.ppermute(first, axis, down)
        shard = jnp.concatenate([before, shard, after], axis=dim)
    return shard


def cut_along(shard, dim, peers):
    before, after = (shard.shape[:dim], shard.shape[dim + 1 :])
    return jnp.moveaxis(shard.reshape(*before, peers, -1, *after), dim, 0)


def sent_and_summed(shard, axis, dim):
    peers = lax.axis_size(axis)
    pieces = lax.all_to_all(cut_along(shard, dim, peers), axis, 0, 0, tiled=True)
    return jnp.sum(pieces.astype(jnp.float32), axis=0)


def block_step(state_in, block_in):
    memory, normal_sum, running_top = state_in
    query_blk, key_blk, value_blk, rate_blk, decay_blk = block_in
    length = decay_blk.shape[-1]
    cumul_decay = jnp.cumsum(decay_blk, axis=-1)
    block_total = cumul_decay[:, -1]
    lower = jnp.arange(length)[:, None] >= jnp.arange(length)[None, :]
    spread = cumul_decay[:, :, None] - cumul_decay[:, None, :] + rate_blk[:, None, :]
    spread = jnp.where(lower[None], spread, -jnp.inf)
    carried = cumul_decay + running_top[:, None]
    row_top = jnp.maximum(carried, jnp.max(spread, axis=-1))
    carry_weight = jnp.exp(carried - row_top)
    scores = jnp.einsum("hid,hjd->hij", query_blk, key_blk, precision=precise_mode) * jnp.exp(
        spread - row_top[:, :, None]
    )
    numer = jnp.einsum("hij,hje->hie", scores, value_blk, precision=precise_mode)
    numer = numer + carry_weight[:, :, None] * jnp.einsum(
        "hid,hde->hie", query_blk, memory, precision=precise_mode
    )
    denom = jnp.sum(scores, axis=-1) + carry_weight * jnp.einsum(
        "hid,hd->hi", query_blk, normal_sum, precision=precise_mode
    )
    output = numer / jnp.maximum(jnp.abs(denom), jnp.exp(-row_top))[:, :, None]
    tail_weight = block_total[:, None] - cumul_decay + rate_blk
    new_top = jnp.maximum(block_total + running_top, jnp.max(tail_weight, axis=-1))
    fresh = jnp.exp(tail_weight - new_top[:, None])
    fade = jnp.exp(block_total + running_top - new_top)
    memory = fade[:, None, None] * memory + jnp.einsum(
        "hjd,hje->hde", key_blk * fresh[:, :, None], value_blk, precision=precise_mode
    )
    normal_sum = fade[:, None] * normal_sum + jnp.einsum(
        "hj,hjd->hd", fresh, key_blk, precision=precise_mode
    )
    return ((memory, normal_sum, new_top), output)


def run_blocks(query_heads, key_heads, value_heads, rate, decay, start_state):
    heads = query_heads.shape[0]
    length = query_heads.shape[1]
    count = length // BLOCK

    def to_blocks(array):
        return jnp.moveaxis(array.reshape((heads, count, BLOCK) + array.shape[2:]), 1, 0)

    inputs = tuple(
        (to_blocks(array) for array in (query_heads, key_heads, value_heads, rate, decay))
    )
    _, outputs = lax.scan(block_step, start_state, inputs)
    return jnp.moveaxis(outputs, 0, 1).reshape(heads, length, -1)


def summarize(key_heads, value_heads, rate, decay):
    cumul_decay = jnp.cumsum(decay, axis=-1)
    chain_total = cumul_decay[:, -1]
    tail_weight = chain_total[:, None] - cumul_decay + rate
    chain_top = jnp.max(tail_weight, axis=-1)
    fresh = jnp.exp(tail_weight - chain_top[:, None])
    memory = jnp.einsum(
        "hjd,hje->hde", key_heads * fresh[:, :, None], value_heads, precision=precise_mode
    )
    normal_sum = jnp.einsum("hj,hjd->hd", fresh, key_heads, precision=precise_mode)
    return (chain_total, memory, normal_sum, chain_top)


def combine(earlier, later):
    total_a, memory_a, normal_a, top_a = earlier
    total_b, memory_b, normal_b, top_b = later
    lifted = total_b + top_a
    joint_top = jnp.maximum(lifted, top_b)
    weight_a = jnp.exp(lifted - joint_top)
    weight_b = jnp.exp(top_b - joint_top)
    memory = weight_a[:, None, None] * memory_a + weight_b[:, None, None] * memory_b
    normal_sum = weight_a[:, None] * normal_a + weight_b[:, None] * normal_b
    return (total_a + total_b, memory, normal_sum, joint_top)


def body(
    lookup_request_vectors,
    lookup_address_vectors,
    lookup_content_vectors,
    admission_preactivation,
    retention_preactivation,
    extra_decay_terms,
    per_slot_rescale_factor,
    mixer_exit_matrix,
    skip_path_activity,
    mlp_rescale_factor,
    filter_widening_matrix,
    multiplier_widening_matrix,
    neighbour_filter_coefficients,
    contracting_matrix,
):
    row_count = lookup_request_vectors.shape[0]
    local_heads = admission_preactivation.shape[1]

    def split_heads(array):
        return (
            array.astype(jnp.float32).reshape(row_count, local_heads, HEAD_DIM).transpose(1, 0, 2)
        )

    query_heads = split_heads(lookup_request_vectors)
    key_heads = split_heads(lookup_address_vectors) * HEAD_DIM ** (-0.5)
    value_heads = split_heads(lookup_content_vectors)
    retention_log_share = jax.nn.log_sigmoid(retention_preactivation) + extra_decay_terms
    back_query = jnp.flip(query_heads, 1)
    back_key = jnp.flip(key_heads, 1)
    back_value = jnp.flip(value_heads, 1)
    back_rate = jnp.flip(admission_preactivation[1], 1)
    back_decay = jnp.flip(retention_log_share[1], 1)
    identity = (
        jnp.zeros((local_heads,), jnp.float32),
        jnp.zeros((local_heads, HEAD_DIM, HEAD_DIM), jnp.float32),
        jnp.zeros((local_heads, HEAD_DIM), jnp.float32),
        jnp.full((local_heads,), far_below, jnp.float32),
    )
    forward_summary = summarize(
        key_heads, value_heads, admission_preactivation[0], retention_log_share[0]
    )
    backward_summary = summarize(back_key, back_value, back_rate, back_decay)
    forward_in = prefix_by_axis(forward_summary, SP, combine, identity, False)
    backward_in = prefix_by_axis(backward_summary, SP, combine, identity, True)
    forward_out = run_blocks(
        query_heads,
        key_heads,
        value_heads,
        admission_preactivation[0],
        retention_log_share[0],
        forward_in[1:],
    )
    backward_out = run_blocks(
        back_query, back_key, back_value, back_rate, back_decay, backward_in[1:]
    )
    summed = forward_out + jnp.flip(backward_out, 1)
    scaled = summed * lax.rsqrt(jnp.mean(summed * summed, axis=-1, keepdims=True) + epsilon)
    scaled = scaled * per_slot_rescale_factor.reshape(local_heads, HEAD_DIM)[:, None, :]
    mixed = (
        scaled.transpose(1, 0, 2).reshape(row_count, local_heads * HEAD_DIM).astype(jnp.bfloat16)
    )
    token_rows = lax.all_to_all(mixed, "tp", split_axis=0, concat_axis=1, tiled=True)
    whole_out = lax.all_gather(mixer_exit_matrix, "tp", axis=0, tiled=True)
    projected = jnp.dot(token_rows, whole_out, preferred_element_type=jnp.float32)
    middle = (skip_path_activity.astype(jnp.float32) + projected).astype(jnp.bfloat16)
    middle_wide = middle.astype(jnp.float32)
    normed = middle_wide * lax.rsqrt(
        jnp.mean(middle_wide * middle_wide, axis=-1, keepdims=True) + epsilon
    )
    normed = (normed * mlp_rescale_factor).astype(jnp.bfloat16)
    token_block = collect(normed, "tp", 0)
    pieces = side_by_side((filter_widening_matrix, multiplier_widening_matrix), SP, 0, 1)
    inner_sum = jnp.dot(token_block, pieces[0], preferred_element_type=jnp.float32)
    gate_sum = jnp.dot(token_block, pieces[1], preferred_element_type=jnp.float32)
    inner = inner_sum.astype(jnp.bfloat16)
    edged = extended(inner, ((SP, 0),), 1).astype(jnp.float32)
    conv = (
        neighbour_filter_coefficients[0] * edged[:-2]
        + neighbour_filter_coefficients[1] * edged[1:-1]
        + neighbour_filter_coefficients[2] * edged[2:]
    )
    hidden = (jax.nn.gelu(conv) * gate_sum).astype(jnp.bfloat16)
    whole_down = lax.all_gather(contracting_matrix, SP, axis=1, tiled=True)
    lowered = sent_and_summed(
        jnp.dot(hidden, whole_down, preferred_element_type=jnp.float32).astype(jnp.bfloat16),
        "tp",
        0,
    )
    return (middle_wide + lowered).astype(jnp.bfloat16)


def solution(mesh):
    split = Mesh(mesh.devices.reshape(8, 8, mesh.shape["tp"]), ("sp_0", "sp_1", "tp"))
    placed = (
        P(SP, "tp"),
        P(SP, "tp"),
        P(SP, "tp"),
        P(None, "tp", SP),
        P(None, "tp", SP),
        P(None, "tp", SP),
        P("tp"),
        P("tp", None),
        P(SP_TP, None),
        P(),
        P(SP, "tp"),
        P(SP, "tp"),
        P(None, "tp"),
        P("tp", SP),
    )
    return jax.shard_map(
        body, mesh=split, in_specs=placed, out_specs=P(SP_TP, None), check_vma=False
    )
```

profile of v0, /device:TPU:1, one launch (start us, length us, event | category | flops | bytes accessed | tf_op | source)
XLA Modules:
  0.0 268.8 jit_solution(16417950721852467293)
XLA Ops:
  6.5 0.7 all-gather.12.cloned.1.call-update
  7.3 1.5 pad_maximum_fusion
  8.9 0.7 all-gather.16.cloned.1.call-update
  9.6 0.7 fusion.97
  10.3 0.5 slice_bitcast_fusion.2
  11.1 0.6 reduce-window.16
  12.3 0.6 reduce-window.14
  13.5 1.3 slice_bitcast_fusion.4
  15.0 0.9 fusion.196
  16.0 0.9 copy.528
  16.9 0.9 copy.530
  18.8 23.0 %all-gather.4 = f32[8,132,64]{1,2,0:T(8,128)S(1)} all-gather(f32[1,132,64]{1,2,0:T(8,128)S(1)} %maximum_bitcast_fusion), channel_id=2, replica_groups=mesh['sp_0'=8,'sp_1'=8,'tp'=8] {'sp_1'}, dimensions={0}, use_global_device_ids=true | all-gather | bytes 304128 | tf_op jit(solution)/shard_map/all_gather | solution.py:32
  42.4 0.4 copy-done.87
  42.9 0.6 bitcast_add_fusion.32
  46.7 0.7 fusion.135
  47.5 0.5 copy-done.15
  48.5 26.4 %all-gather.5 = f32[8,132,64]{1,2,0:T(8,128)S(1)} all-gather(f32[1,132,64]{1,2,0:T(8,128)S(1)} %maximum_bitcast_fusion.1), channel_id=3, replica_groups=mesh['sp_0'=8,'sp_1'=8,'tp'=8] {'sp_0'}, dimensions={0}, use_global_device_ids=true | all-gather | bytes 304128 | tf_op jit(solution)/shard_map/all_gather | solution.py:32
  75.0 0.7 fusion.204
  77.4 20.8 %all-gather.6 = f32[8,132,64]{1,2,0:T(8,128)S(1)} all-gather(f32[1,132,64]{1,2,0:T(8,128)S(1)} %maximum_bitcast_fusion.2), channel_id=4, replica_groups=mesh['sp_0'=8,'sp_1'=8,'tp'=8] {'sp_1'}, dimensions={0}, use_global_device_ids=true | all-gather | bytes 304128 | tf_op jit(solution)/shard_map/all_gather | solution.py:32
  98.8 0.4 copy-done.77
  99.5 0.5 bitcast_add_fusion.10
  103.1 0.7 fusion.116
  104.5 22.1 %all-gather.7 = f32[8,132,64]{1,2,0:T(8,128)S(1)} all-gather(f32[1,132,64]{1,2,0:T(8,128)S(1)} %maximum_bitcast_fusion.3), channel_id=5, replica_groups=mesh['sp_0'=8,'sp_1'=8,'tp'=8] {'sp_0'}, dimensions={0}, use_global_device_ids=true | all-gather | bytes 304128 | tf_op jit(solution)/shard_map/all_gather | solution.py:32
  127.2 0.9 copy.573
  128.7 0.8 copy.565
  129.6 0.8 copy.566
  130.4 0.8 copy.567
  131.2 0.8 copy.568
  132.1 0.8 copy.569
  132.9 0.8 copy.570
  133.7 0.8 copy.571
  134.6 0.8 copy.572
  137.1 0.8 fusion.181
  138.0 0.9 fusion.127
  138.9 1.1 multiply_add_fusion.3
  140.3 8.6 %while.32 = (s32[]{:T(128)}, f32[2,64,64]{2,1,0:T(8,128)S(1)}, f32[2,64]{1,0:T(2,128)S(1)}, f32[2]{0:T(128)S(1)}, f32[2,2,128,64]{2,3,1,0:T(8,128)S(1)}, /*index...) while((s32[]{:T(128)}, f32[2,64,64]{2,1,0:T(8,128)S(1)}, ...), condition=%wide.region_8.9_spmd, body=%wide.region_3.8_spmd.sunk | while | flops 76352256 | bytes 1591037 | solution.py:152
  140.3 0.6 fusion.307
  140.9 0.3 reduce_window_sum.54
  141.4 0.9 fusion.308
  142.7 0.4 fusion.311
  143.7 0.3 fusion.314
  144.6 0.6 fusion.307
  145.2 0.3 reduce_window_sum.54
  145.7 0.9 fusion.308
  147.0 0.4 fusion.311
  152.5 6.0 %while.33 = (s32[]{:T(128)}, f32[2,64,64]{2,1,0:T(8,128)S(1)}, f32[2,64]{1,0:T(2,128)S(1)}, f32[2]{0:T(128)S(1)}, f32[2,2,128,64]{2,3,1,0:T(8,128)S(1)}, /*index...) while((s32[]{:T(128)}, f32[2,64,64]{2,1,0:T(8,128)S(1)}, ...), condition=%wide.region_17.18_spmd, body=%wide.region_12.17_spmd.sunk | while | flops 76352256 | bytes 1591037 | solution.py:152
  152.5 0.3 reduce_window_sum.55
  153.7 0.4 fusion.331
  155.5 0.3 reduce_window_sum.55
  156.7 0.4 fusion.331
  157.6 0.3 fusion.334
  159.2 29.5 %all_to_all.26 = bf16[8,32,128]{2,1,0:T(8,128)(2,1)S(1)} all-to-all(bf16[8,32,128]{2,1,0:T(8,128)(2,1)S(1)} %convert_element_type.55), channel_id=1, replica_groups=mesh['sp_0'=8,'sp_1'=8,'tp'=8] {'tp'}, dimensions={0} | all-to-all | bytes 131072 | tf_op jit(solution)/shard_map/all_to_all | solution.py:243
  188.8 3.1 %multiply_reduce_fusion = (f32[32]{0:T(128)S(1)}, f32[32,2048]{1,0:T(8,128)S(1)}) fusion(bf16[1024,2048]{1,0:T(8,128)(2,1)} %all-gather.12.cloned.1.call-done, bf16[32,2048]{1,0:T(8,128)(2,1)S(1)} %copy-done, bf16[8,32,128]{2,1,0:T(8,128)(2,1)S(1)} %all_to_all.26), kind=kOutput, calls=%fused_computation.89 | convolution fusion | flops 134610912 | bytes 4653184 | tf_op jit(solution)/shard_map/dot_general | solution.py:245
  192.1 18.1 %all_to_all.27 = bf16[8,32,2048]{2,1,0:T(8,128)(2,1)S(1)} all-to-all(bf16[8,32,2048]{2,1,0:T(8,128)(2,1)S(1)} %broadcast_in_dim.30), channel_id=1, replica_groups=mesh['sp_0'=8,'sp_1'=8,'tp'=8] {'tp'}, dimensions={0} | all-to-all | bytes 2097152 | tf_op jit(solution)/shard_map/all_to_all | solution.py:58
  210.3 3.3 %fusion.30 = bf16[256,704]{0,1:T(8,128)(2,1)S(1)} fusion(bf16[256,2048]{1,0:T(8,128)(2,1)S(1)} %bitcast.1268, bf16[2048,1408]{1,0:T(8,128)(2,1)} %all-gather.14.cloned.1.call-done), kind=kOutput, calls=%fused_computation.65 | convolution fusion | flops 738377728 | bytes 4554752 | tf_op jit(solution)/shard_map/dot_general | solution.py:254
  213.7 2.8 %collective-permute-start = (bf16[1,704]{0,1:T(8,128)(2,1)S(1)}, bf16[1,704]{0,1:T(8,128)(2,1)S(1)}, u32[]{:S(2)}, u32[]{:S(2)}) collective-permute-start(bf16[1,704]{0,1:T(8,128)(2,1)S(1)} %get-tuple-element.424), channel_id=1, source_target_pairs={{0,8},{8,16},{16,24},{24,32},{32,40},{40,48},{48,56},{56,64},{64,7... | collective-permute-start | bytes 4232 | tf_op jit(solution)/shard_map/ppermute | solution.py:88
  216.5 1.5 collective-permute-start.1
  218.0 5.7 %collective-permute-done = bf16[1,704]{0,1:T(8,128)(2,1)S(1)} collective-permute-done((bf16[1,704]{0,1:T(8,128)(2,1)S(1)}, bf16[1,704]{0,1:T(8,128)(2,1)S(1)}, u32[]{:S(2)}, u32[]{:S(2)}) %collective-permute-start) | collective-permute-done | bytes 1440 | tf_op jit(solution)/shard_map/ppermute | solution.py:88
  223.7 3.7 %collective-permute-done.1 = bf16[1,704]{0,1:T(8,128)(2,1)S(1)} collective-permute-done((bf16[1,704]{0,1:T(8,128)(2,1)S(1)}, bf16[1,704]{0,1:T(8,128)(2,1)S(1)}, u32[]{:S(2)}, u32[]{:S(2)}) %collective-permute-start.1) | collective-permute-done | bytes 1440 | tf_op jit(solution)/shard_map/ppermute | solution.py:89
  227.5 0.3 maximum_convert_fusion
  227.8 2.0 all-gather.16.cloned.1.call-done
  229.8 7.9 %convolution_convert_fusion = bf16[256,2048]{1,0:T(8,128)(2,1)S(1)} fusion(bf16[704,2048]{0,1:T(8,128)(2,1)} %all-gather.16.cloned.1.call-done, bf16[256,2048]{1,0:T(8,128)(2,1)S(1)} %bitcast.1269, bf16[2048,1408]{1,0:T(8,128)(2,1)} %all-gather.14.cloned.1.call-done, f32[258,704]{0,1:T(8,128)S(1)} %maximum_convert_fusion, f32[704]{0:T(1024)S(1)} %get-tuple-element.232, ...), kind=kOutput, calls=%fused_computation.58 | convolution fusion | flops 1479622656 | bytes 10563584 | tf_op jit(solution)/shard_map/dot_general | solution.py:266
  237.6 23.8 %all_to_all.28 = bf16[8,32,2048]{2,1,0:T(8,128)(2,1)S(1)} all-to-all(bf16[8,32,2048]{2,1,0:T(8,128)(2,1)S(1)} %bitcast.1270), channel_id=1, replica_groups=mesh['sp_0'=8,'sp_1'=8,'tp'=8] {'tp'}, dimensions={0} | all-to-all | bytes 2097152 | tf_op jit(solution)/shard_map/all_to_all | solution.py:101
  261.6 0.7 add_convert_fusion
  (486 shorter events, 27.8 us)
Async XLA Ops:
  6.5 182.2 %all-gather.12.cloned.1.call-start = ((), (), s32[]{:S(2)}) async-start(), calls=%async_computation.3 | async-start | bytes 4718592 | tf_op jit(solution)/shard_map/all_gather | solution.py:244
  7.3 203.0 %all-gather.14.cloned.1.call-start = ((), (), s32[]{:S(2)}) async-start(), calls=%async_computation.4 | async-start | bytes 5857280 | tf_op jit(solution)/shard_map/all_gather | solution.py:78
  8.9 220.9 %all-gather.16.cloned.1.call-start = ((), (), s32[]{:S(2)}) async-start(), calls=%async_computation.5 | async-start | bytes 3194880 | tf_op jit(solution)/shard_map/all_gather | solution.py:264
  42.8 5.4 %copy-start.70 = (f32[2]{0:T(128)}, f32[2]{0:T(128)S(1)}, u32[]{:S(2)}) copy-start(f32[2]{0:T(128)S(1)} %get-tuple-element.482) | copy-start | bytes 28
  98.8 27.9 %copy-start.16 = (f32[2]{0:T(128)}, f32[2]{0:T(128)S(1)}, u32[]{:S(2)}) copy-start(f32[2]{0:T(128)S(1)} %get-tuple-element.330) | copy-start | bytes 28
  99.3 27.3 %copy-start.18 = (f32[2]{0:T(128)}, f32[2]{0:T(128)S(1)}, u32[]{:S(2)}) copy-start(f32[2]{0:T(128)S(1)} %get-tuple-element.467) | copy-start | bytes 28
  99.3 27.3 %copy-start.20 = (f32[2]{0:T(128)}, f32[2]{0:T(128)S(1)}, u32[]{:S(2)}) copy-start(f32[2]{0:T(128)S(1)} %get-tuple-element.469) | copy-start | bytes 28
  99.3 27.3 %copy-start.22 = (f32[2]{0:T(128)}, f32[2]{0:T(128)S(1)}, u32[]{:S(2)}) copy-start(f32[2]{0:T(128)S(1)} %get-tuple-element.471) | copy-start | bytes 28
  99.3 27.3 %copy-start.24 = (f32[2]{0:T(128)}, f32[2]{0:T(128)S(1)}, u32[]{:S(2)}) copy-start(f32[2]{0:T(128)S(1)} %get-tuple-element.472) | copy-start | bytes 28
  99.3 27.4 %copy-start.26 = (f32[2]{0:T(128)}, f32[2]{0:T(128)S(1)}, u32[]{:S(2)}) copy-start(f32[2]{0:T(128)S(1)} %get-tuple-element.475) | copy-start | bytes 28
  99.3 27.4 %copy-start.51 = (f32[2]{0:T(128)}, f32[2]{0:T(128)S(1)}, u32[]{:S(2)}) copy-start(f32[2]{0:T(128)S(1)} %get-tuple-element.338) | copy-start | bytes 28
  99.3 27.4 %copy-start.53 = (f32[2]{0:T(128)}, f32[2]{0:T(128)S(1)}, u32[]{:S(2)}) copy-start(f32[2]{0:T(128)S(1)} %get-tuple-element.468) | copy-start | bytes 28
  99.3 27.4 %copy-start.55 = (f32[2]{0:T(128)}, f32[2]{0:T(128)S(1)}, u32[]{:S(2)}) copy-start(f32[2]{0:T(128)S(1)} %get-tuple-element.470) | copy-start | bytes 28
  99.3 27.4 %copy-start.57 = (f32[2]{0:T(128)}, f32[2]{0:T(128)S(1)}, u32[]{:S(2)}) copy-start(f32[2]{0:T(128)S(1)} %get-tuple-element.473) | copy-start | bytes 28
  99.4 27.4 %copy-start.59 = (f32[2]{0:T(128)}, f32[2]{0:T(128)S(1)}, u32[]{:S(2)}) copy-start(f32[2]{0:T(128)S(1)} %get-tuple-element.474) | copy-start | bytes 28
  99.4 27.4 %copy-start.61 = (f32[2]{0:T(128)}, f32[2]{0:T(128)S(1)}, u32[]{:S(2)}) copy-start(f32[2]{0:T(128)S(1)} %get-tuple-element.476) | copy-start | bytes 28
  99.4 27.4 %copy-start.83 = (f32[2]{0:T(128)}, f32[2]{0:T(128)S(1)}, u32[]{:S(2)}) copy-start(f32[2]{0:T(128)S(1)} %get-tuple-element.339) | copy-start | bytes 28
  99.4 27.3 %copy-start.28 = (f32[2]{0:T(128)}, f32[2]{0:T(128)S(1)}, u32[]{:S(2)}) copy-start(f32[2]{0:T(128)S(1)} %get-tuple-element.499) | copy-start | bytes 28
  99.4 27.3 %copy-start.30 = (f32[2]{0:T(128)}, f32[2]{0:T(128)S(1)}, u32[]{:S(2)}) copy-start(f32[2]{0:T(128)S(1)} %get-tuple-element.502) | copy-start | bytes 28
  99.4 27.3 %copy-start.63 = (f32[2]{0:T(128)}, f32[2]{0:T(128)S(1)}, u32[]{:S(2)}) copy-start(f32[2]{0:T(128)S(1)} %get-tuple-element.500) | copy-start | bytes 28
  99.4 27.3 %copy-start.65 = (f32[2]{0:T(128)}, f32[2]{0:T(128)S(1)}, u32[]{:S(2)}) copy-start(f32[2]{0:T(128)S(1)} %get-tuple-element.501) | copy-start | bytes 28
  102.5 24.3 %copy-start.1 = (f32[1,2,64]{2,1,0:T(2,128)}, f32[1,2,64]{2,1,0:T(2,128)S(1)}, u32[]{:S(2)}) copy-start(f32[1,2,64]{2,1,0:T(2,128)S(1)} %copy.584) | copy-start | bytes 1540
  102.6 24.2 %copy-start.3 = (f32[1,2,64]{2,1,0:T(2,128)}, f32[1,2,64]{2,1,0:T(2,128)S(1)}, u32[]{:S(2)}) copy-start(f32[1,2,64]{2,1,0:T(2,128)S(1)} %copy.586) | copy-start | bytes 1540
  102.7 24.1 %copy-start.5 = (f32[1,2,64]{2,1,0:T(2,128)}, f32[1,2,64]{2,1,0:T(2,128)S(1)}, u32[]{:S(2)}) copy-start(f32[1,2,64]{2,1,0:T(2,128)S(1)} %copy.588) | copy-start | bytes 1540
  102.8 24.0 %copy-start.7 = (f32[1,2,64]{2,1,0:T(2,128)}, f32[1,2,64]{2,1,0:T(2,128)S(1)}, u32[]{:S(2)}) copy-start(f32[1,2,64]{2,1,0:T(2,128)S(1)} %copy.590) | copy-start | bytes 1540
  140.0 11.6 %copy-start.42 = (f32[2]{0:T(128)S(1)}, f32[2]{0:T(128)}, u32[]{:S(2)}) copy-start(f32[2]{0:T(128)} %copy-done.41) | copy-start | bytes 28
  140.0 11.6 %copy-start.44 = (f32[2]{0:T(128)S(1)}, f32[2]{0:T(128)}, u32[]{:S(2)}) copy-start(f32[2]{0:T(128)} %copy-done.43) | copy-start | bytes 28
  140.0 11.6 %copy-start.46 = (f32[2]{0:T(128)S(1)}, f32[2]{0:T(128)}, u32[]{:S(2)}) copy-start(f32[2]{0:T(128)} %copy-done.45) | copy-start | bytes 28
  140.0 11.6 %copy-start.76 = (f32[2]{0:T(128)S(1)}, f32[2]{0:T(128)}, u32[]{:S(2)}) copy-start(f32[2]{0:T(128)} %copy-done.75) | copy-start | bytes 28
  140.0 11.6 %copy-start.78 = (f32[2]{0:T(128)S(1)}, f32[2]{0:T(128)}, u32[]{:S(2)}) copy-start(f32[2]{0:T(128)} %copy-done.77) | copy-start | bytes 28
  140.0 11.6 %copy-start.80 = (f32[2]{0:T(128)S(1)}, f32[2]{0:T(128)}, u32[]{:S(2)}) copy-start(f32[2]{0:T(128)} %copy-done.79) | copy-start | bytes 28
  140.0 11.6 %copy-start.82 = (f32[2]{0:T(128)S(1)}, f32[2]{0:T(128)}, u32[]{:S(2)}) copy-start(f32[2]{0:T(128)} %copy-done.81) | copy-start | bytes 28
  140.0 11.6 %copy-start.84 = (f32[2]{0:T(128)S(1)}, f32[2]{0:T(128)}, u32[]{:S(2)}) copy-start(f32[2]{0:T(128)} %copy-done.83) | copy-start | bytes 28
  140.0 11.6 %copy-start.93 = (f32[2]{0:T(128)S(1)}, f32[2]{0:T(128)}, u32[]{:S(2)}) copy-start(f32[2]{0:T(128)} %get-tuple-element.341) | copy-start | bytes 28
  140.1 11.7 %copy-start.2 = (f32[1,2,64]{2,1,0:T(2,128)S(1)}, f32[1,2,64]{2,1,0:T(2,128)}, u32[]{:S(2)}) copy-start(f32[1,2,64]{2,1,0:T(2,128)} %copy-done.1) | copy-start | bytes 1540
  140.1 11.7 %copy-start.4 = (f32[1,2,64]{2,1,0:T(2,128)S(1)}, f32[1,2,64]{2,1,0:T(2,128)}, u32[]{:S(2)}) copy-start(f32[1,2,64]{2,1,0:T(2,128)} %copy-done.3) | copy-start | bytes 1540
  140.1 11.7 %copy-start.6 = (f32[1,2,64]{2,1,0:T(2,128)S(1)}, f32[1,2,64]{2,1,0:T(2,128)}, u32[]{:S(2)}) copy-start(f32[1,2,64]{2,1,0:T(2,128)} %copy-done.5) | copy-start | bytes 1540
  140.1 11.7 %copy-start.8 = (f32[1,2,64]{2,1,0:T(2,128)S(1)}, f32[1,2,64]{2,1,0:T(2,128)}, u32[]{:S(2)}) copy-start(f32[1,2,64]{2,1,0:T(2,128)} %copy-done.7) | copy-start | bytes 1540
  140.1 11.7 %copy-start.10 = (f32[2,64]{1,0:T(2,128)S(1)}, f32[2,64]{1,0:T(2,128)}, u32[]{:S(2)}) copy-start(f32[2,64]{1,0:T(2,128)} %copy-done.9) | copy-start | bytes 1540
  140.1 11.7 %copy-start.17 = (f32[2]{0:T(128)S(1)}, f32[2]{0:T(128)}, u32[]{:S(2)}) copy-start(f32[2]{0:T(128)} %copy-done.16) | copy-start | bytes 28
  140.1 11.7 %copy-start.19 = (f32[2]{0:T(128)S(1)}, f32[2]{0:T(128)}, u32[]{:S(2)}) copy-start(f32[2]{0:T(128)} %copy-done.18) | copy-start | bytes 28
  140.1 11.7 %copy-start.21 = (f32[2]{0:T(128)S(1)}, f32[2]{0:T(128)}, u32[]{:S(2)}) copy-start(f32[2]{0:T(128)} %copy-done.20) | copy-start | bytes 28
  140.1 11.7 %copy-start.23 = (f32[2]{0:T(128)S(1)}, f32[2]{0:T(128)}, u32[]{:S(2)}) copy-start(f32[2]{0:T(128)} %copy-done.22) | copy-start | bytes 28
  140.1 11.7 %copy-start.25 = (f32[2]{0:T(128)S(1)}, f32[2]{0:T(128)}, u32[]{:S(2)}) copy-start(f32[2]{0:T(128)} %copy-done.24) | copy-start | bytes 28
  140.2 11.7 %copy-start.27 = (f32[2]{0:T(128)S(1)}, f32[2]{0:T(128)}, u32[]{:S(2)}) copy-start(f32[2]{0:T(128)} %copy-done.26) | copy-start | bytes 28
  140.2 11.7 %copy-start.29 = (f32[2]{0:T(128)S(1)}, f32[2]{0:T(128)}, u32[]{:S(2)}) copy-start(f32[2]{0:T(128)} %copy-done.28) | copy-start | bytes 28
  140.2 11.7 %copy-start.31 = (f32[2]{0:T(128)S(1)}, f32[2]{0:T(128)}, u32[]{:S(2)}) copy-start(f32[2]{0:T(128)} %copy-done.30) | copy-start | bytes 28
  140.2 11.7 %copy-start.90 = (f32[2,64]{1,0:T(2,128)S(1)}, f32[2,64]{1,0:T(2,128)}, u32[]{:S(2)}) copy-start(f32[2,64]{1,0:T(2,128)} %get-tuple-element.327) | copy-start | bytes 1540
  140.2 11.7 %copy-start.91 = (f32[2,64]{1,0:T(2,128)S(1)}, f32[2,64]{1,0:T(2,128)}, u32[]{:S(2)}) copy-start(f32[2,64]{1,0:T(2,128)} %get-tuple-element.328) | copy-start | bytes 1540
  140.2 11.7 %copy-start.92 = (f32[2,64]{1,0:T(2,128)S(1)}, f32[2,64]{1,0:T(2,128)}, u32[]{:S(2)}) copy-start(f32[2,64]{1,0:T(2,128)} %get-tuple-element.329) | copy-start | bytes 1540
  140.2 11.9 %copy-start.52 = (f32[2]{0:T(128)S(1)}, f32[2]{0:T(128)}, u32[]{:S(2)}) copy-start(f32[2]{0:T(128)} %copy-done.51) | copy-start | bytes 28
  140.2 11.9 %copy-start.54 = (f32[2]{0:T(128)S(1)}, f32[2]{0:T(128)}, u32[]{:S(2)}) copy-start(f32[2]{0:T(128)} %copy-done.53) | copy-start | bytes 28
  140.2 11.9 %copy-start.56 = (f32[2]{0:T(128)S(1)}, f32[2]{0:T(128)}, u32[]{:S(2)}) copy-start(f32[2]{0:T(128)} %copy-done.55) | copy-start | bytes 28
  140.2 11.9 %copy-start.58 = (f32[2]{0:T(128)S(1)}, f32[2]{0:T(128)}, u32[]{:S(2)}) copy-start(f32[2]{0:T(128)} %copy-done.57) | copy-start | bytes 28
  140.3 11.9 %copy-start.60 = (f32[2]{0:T(128)S(1)}, f32[2]{0:T(128)}, u32[]{:S(2)}) copy-start(f32[2]{0:T(128)} %copy-done.59) | copy-start | bytes 28
  140.3 11.9 %copy-start.62 = (f32[2]{0:T(128)S(1)}, f32[2]{0:T(128)}, u32[]{:S(2)}) copy-start(f32[2]{0:T(128)} %copy-done.61) | copy-start | bytes 28
  140.3 11.9 %copy-start.64 = (f32[2]{0:T(128)S(1)}, f32[2]{0:T(128)}, u32[]{:S(2)}) copy-start(f32[2]{0:T(128)} %copy-done.63) | copy-start | bytes 28
  140.3 11.9 %copy-start.66 = (f32[2]{0:T(128)S(1)}, f32[2]{0:T(128)}, u32[]{:S(2)}) copy-start(f32[2]{0:T(128)} %copy-done.65) | copy-start | bytes 28
  152.5 6.3 %copy-start.94 = (f32[128]{0:T(128)S(1)}, f32[128]{0:T(128)}, u32[]{:S(2)}) copy-start(f32[128]{0:T(128)} %param.24) | copy-start | bytes 1540
  152.5 36.3 %copy-start = (bf16[32,2048]{1,0:T(8,128)(2,1)S(1)}, bf16[32,2048]{1,0:T(8,128)(2,1)}, u32[]{:S(2)}) copy-start(bf16[32,2048]{1,0:T(8,128)(2,1)} %param.26) | copy-start | bytes 393220
  158.5 33.4 %copy-start.40 = (f32[2048]{0:T(1024)S(1)}, f32[2048]{0:T(1024)}, u32[]{:S(2)}) copy-start(f32[2048]{0:T(1024)} %param.27) | copy-start | bytes 24580
  210.3 7.7 %copy-start.50 = (f32[3,704]{1,0:T(4,128)S(1)}, f32[3,704]{1,0:T(4,128)}, u32[]{:S(2)}) copy-start(f32[3,704]{1,0:T(4,128)} %param.30) | copy-start | bytes 25348
  213.7 10.1 %collective-permute-start = (bf16[1,704]{0,1:T(8,128)(2,1)S(1)}, bf16[1,704]{0,1:T(8,128)(2,1)S(1)}, u32[]{:S(2)}, u32[]{:S(2)}) collective-permute-start(bf16[1,704]{0,1:T(8,128)(2,1)S(1)} %get-tuple-element.424), channel_id=1, source_target_pairs={{0,8},{8,16},{16,24},{24,32},{32,40},{40,48},{48,56},{56,64},{64,7... | collective-permute-start | bytes 4232 | tf_op jit(solution)/shard_map/ppermute | solution.py:88
  216.5 11.0 %collective-permute-start.1 = (bf16[1,704]{0,1:T(8,128)(2,1)S(1)}, bf16[1,704]{0,1:T(8,128)(2,1)S(1)}, u32[]{:S(2)}, u32[]{:S(2)}) collective-permute-start(bf16[1,704]{0,1:T(8,128)(2,1)S(1)} %get-tuple-element.425), channel_id=1, source_target_pairs={{8,0},{16,8},{24,16},{32,24},{40,32},{48,40},{56,48},{64,56},{72,6... | collective-permute-start | bytes 4232 | tf_op jit(solution)/shard_map/ppermute | solution.py:89
  (36 other events, 121.3 us)
Sparse Core Ops, SparseCore 0:
  9.5 43.2 all-gather.11
  55.8 90.1 all-gather.13
  149.0 80.7 all-gather.15
where the time goes:
time: 270 us; the launch traced here: 269 us
  blocking collectives  164 us (61%)
  local copies, waits for them, and re-layouts  32.9 us (12%)
  matrix products  21.5 us (8%)
  other arithmetic  18.1 us (7%)
  between operations  15.2 us (6%)
  waiting for transfers between devices  12.9 us (5%)
  starting transfers between devices  4.38 us (2%)
    all_gather x4, blocking collectives, gathered_once(): both, at, found = (lax.all_gather(jnp.concatenate(lines), axis), 0, {})  92.2 us
    all_to_all x1, blocking collectives, body(): lax.all_to_all(mixed, 'tp', split_axis=0, concat_axis=1, tiled=True)  29.5 us
    all_to_all x1, blocking collectives, sent_and_summed(): lax.all_to_all(cut_along(shard, dim, peers), axis, 0, 0, tiled=True)  23.8 us
    all_to_all x1, blocking collectives, from_everyone(): return lax.all_to_all(copies, axis, split_axis=0, concat_axis=0, tiled=True)  18.1 us
    slice x40, local copies, waits for them, and re-layouts, prefix_by_axis(): running = combine(running, jax.tree.map(lambda part: part[k], pieces))  9.36 us
    dot_general x1, matrix products, body(): jnp.dot(hidden, whole_down, preferred_element_type=jnp.float32)  7.85 us
    unnamed x203, local copies, waits for them, and re-layouts  5.96 us
    ppermute x1, waiting for transfers between devices, extended(): before = lax.ppermute(last, axis, up)  5.72 us
  transfers between devices with their start and end apart: 5, of which 3 were waited for; matrix products, arithmetic and copies ran while one was open for 23% of the time, Pallas kernels for 0%

commit v1 on v0

v1 whole, which is shorter than its diff:
```python
import jax
import jax.numpy as jnp
from jax import lax
from jax.experimental import pallas as pl
from jax.experimental.pallas import tpu as pltpu
from jax.sharding import Mesh
from jax.sharding import PartitionSpec as P

HEAD_DIM = 64
SP = ("sp_0", "sp_1")
TP = ("x", "core")
SP_TP = SP + TP
EPS = 1e-06
FAR_BELOW = -1e30
STATE_ROWS = 136
HALF_ROWS = 72
LANES = 128
HIDDEN = 704
MAIN = 640
GATE_AT = MAIN + 128
DOWN_AT = GATE_AT + MAIN
PACKED = DOWN_AT + 768
FEED_STEPS = 4
ANY = pl.BlockSpec(memory_space=pl.ANY)
f32 = jnp.float32
bf16 = jnp.bfloat16
VMEM = pl.BlockSpec(memory_space=pltpu.VMEM)
SMEM = pl.BlockSpec(memory_space=pltpu.SMEM)


def three_parts(x):
    hi = x.astype(bf16)
    rest = x - hi.astype(f32)
    mid = rest.astype(bf16)
    low = (rest - mid.astype(f32)).astype(bf16)
    return hi, mid, low


def dot(a, b, dims=((1,), (0,))):
    return lax.dot_general(a, b, (dims, ((), ())), preferred_element_type=f32)


def dot_parts(parts, b, dims=((1,), (0,))):
    total = dot(parts[0], b, dims)
    for part in parts[1:]:
        total = total + dot(part, b, dims)
    return total


def iota(shape, dim):
    return lax.broadcasted_iota(jnp.int32, shape, dim)


def gate_rows(ref):
    place = iota((8, ref.shape[2]), 0)
    out = jnp.zeros((8, ref.shape[2]), f32)
    for d in range(2):
        for h in range(2):
            out = jnp.where(place == 2 * d + h, ref[d, h : h + 1, :], out)
    return out


def by_head(first, second, shape):
    return jnp.where(iota(shape, len(shape) - 1) < HEAD_DIM, first, second)


def packed_tail(rows):
    place = iota((8, LANES), 0)
    out = jnp.zeros((8, LANES), f32)
    for k, row in enumerate(rows):
        out = jnp.where(place == k, row, out)
    return out


def write_state(out_ref, memories, normals, totals, tops):
    tail = packed_tail([*normals, *totals, *tops])
    for copy in range(out_ref.shape[0]):
        for d in range(2):
            out_ref[copy, 64 * d : 64 * (d + 1), :] = memories[d]
        out_ref[copy, 128:, :] = tail


def write_halves(out_ref, here, memories, normals, totals, tops):
    tails = [packed_tail([normals[d], totals[d], tops[d]]) for d in range(2)]
    for copy in range(out_ref.shape[0]):
        later = copy > here
        out_ref[copy, :64, :] = jnp.where(later, memories[0], memories[1])
        out_ref[copy, 64:, :] = jnp.where(later, tails[0], tails[1])


def read_state(ref, j, d):
    if ref.shape[1] == HALF_ROWS:
        tail, at, step = ref[j, 64:, :], 0, 1
    else:
        tail, at, step = ref[j, 128:, :], d, 2
    return tuple(tail[at + k * step : at + k * step + 1] for k in range(3))


def summarize_kernel(key_ref, value_ref, rate_ref, decay_ref, out_ref):
    length = key_ref.shape[0]
    rate = gate_rows(rate_ref)
    decay = gate_rows(decay_ref)
    upper = (iota((length, length), 0) <= iota((length, length), 1)).astype(bf16)
    cumul = dot_parts(three_parts(decay), upper)
    total = cumul[:, length - 1 : length]
    is_forward = iota((8, length), 0) < 2
    weight = jnp.where(is_forward, total - cumul, cumul - decay) + rate
    top = jnp.max(weight, axis=1, keepdims=True)
    fresh = jnp.exp(weight - top)
    key_t = key_ref[...].astype(f32).T * HEAD_DIM ** (-0.5)
    value = value_ref[...]
    normal_all = dot_parts(three_parts(fresh), key_ref[...]) * HEAD_DIM ** (-0.5)
    memories, normals, totals, tops = [], [], [], []
    for d in range(2):
        a, b = 2 * d, 2 * d + 1
        spread = jnp.concatenate(
            [
                jnp.broadcast_to(fresh[a : a + 1], (HEAD_DIM, length)),
                jnp.broadcast_to(fresh[b : b + 1], (HEAD_DIM, length)),
            ],
            axis=0,
        )
        both = dot_parts(three_parts(key_t * spread), value)
        memories.append(by_head(both[:HEAD_DIM], both[HEAD_DIM:], (HEAD_DIM, LANES)))
        row = (1, LANES)
        normals.append(by_head(normal_all[a : a + 1], normal_all[b : b + 1], row))
        totals.append(by_head(total[a : a + 1], total[b : b + 1], row))
        tops.append(by_head(top[a : a + 1], top[b : b + 1], row))
    write_state(out_ref, memories, normals, totals, tops)


def weigh(entries, order, active):
    row = (1, LANES)
    since = jnp.zeros(row, f32)
    exponents = {}
    for j in order:
        _, total, top = entries[j]
        on = active(j)
        exponents[j] = jnp.where(on, top + since, FAR_BELOW)
        since = since + jnp.where(on, total, 0.0)
    highest = jnp.full(row, FAR_BELOW, f32)
    for j in order:
        highest = jnp.maximum(highest, exponents[j])
    weights = {
        j: jnp.where(active(j), jnp.exp(exponents[j] - highest), 0.0) for j in order
    }
    return weights, since, highest


def gathered(ref, entries, weights, d):
    memory = jnp.zeros((HEAD_DIM, LANES), f32)
    normal = jnp.zeros((1, LANES), f32)
    for j, w in weights.items():
        at = 0 if ref.shape[1] == HALF_ROWS else 64 * d
        memory = memory + w * ref[j, at : at + 64, :]
        normal = normal + w * entries[j][0]
    return memory, normal


def nearest_first(d, peers):
    return list(reversed(range(peers))) if d == 0 else list(range(peers))


def before(d, here):
    return (lambda j: j < here) if d == 0 else (lambda j: j > here)


def combine_kernel(here_ref, pieces_ref, out_ref, inside_ref, inside_tail_ref):
    peers = pieces_ref.shape[0]
    here = here_ref[0]
    memories, normals, totals, tops, tail = [], [], [], [], []
    for d in range(2):
        entries = [read_state(pieces_ref, j, d) for j in range(peers)]
        order = nearest_first(d, peers)
        weights, since, highest = weigh(entries, order, before(d, here))
        memory, normal = gathered(pieces_ref, entries, weights, d)
        inside_ref[64 * d : 64 * (d + 1), :] = memory
        tail += [normal, since, highest]
        weights, since, highest = weigh(entries, order, lambda j: j >= 0)
        memory, normal = gathered(pieces_ref, entries, weights, d)
        memories.append(memory)
        normals.append(normal)
        totals.append(since)
        tops.append(highest)
    inside_tail_ref[...] = packed_tail(tail)
    write_halves(out_ref, here_ref[1], memories, normals, totals, tops)


def head_sums(x, shape):
    first = iota(shape, 1) < HEAD_DIM
    a = jnp.sum(jnp.where(first, x, 0.0), axis=1, keepdims=True)
    b = jnp.sum(jnp.where(first, 0.0, x), axis=1, keepdims=True)
    return a, b


def mix_kernel(
    here_ref,
    pieces_ref,
    inside_ref,
    inside_tail_ref,
    query_ref,
    key_ref,
    value_ref,
    rate_ref,
    decay_ref,
    gain_ref,
    exit_ref,
    out_ref,
):
    peers = pieces_ref.shape[0]
    here = here_ref[0]
    length = query_ref.shape[0]
    wide = (length, LANES)
    query = query_ref[...]
    value = value_ref[...]
    query32 = query.astype(f32)
    rate = gate_rows(rate_ref)
    parts = three_parts(gate_rows(decay_ref))
    square = (length, length)
    row_at, lane_at = iota(square, 0), iota(square, 1)
    lane_head = iota((length, LANES), 1) // HEAD_DIM
    scores = []
    for h in range(2):
        own = jnp.where(lane_head == h, query32, 0.0).astype(bf16)
        scores.append(dot(own, key_ref[...], ((1,), (1,))) * HEAD_DIM ** (-0.5))
    summed = jnp.zeros(wide, f32)
    for d in range(2):
        entries = [read_state(pieces_ref, j, d) for j in range(peers)]
        weights, _, far_top = weigh(entries, nearest_first(d, peers), before(d, here))
        far_memory, far_normal = gathered(pieces_ref, entries, weights, d)
        near_normal = inside_tail_ref[3 * d : 3 * d + 1]
        near_total = inside_tail_ref[3 * d + 1 : 3 * d + 2]
        near_top = inside_tail_ref[3 * d + 2 : 3 * d + 3]
        lifted = near_total + far_top
        top_in = jnp.maximum(lifted, near_top)
        far_weight = jnp.exp(lifted - top_in)
        near_weight = jnp.exp(near_top - top_in)
        memory = far_weight * far_memory + near_weight * inside_ref[64 * d : 64 * (d + 1), :]
        normal = far_weight * far_normal + near_weight * near_normal

        seen = row_at >= lane_at if d == 0 else row_at <= lane_at
        seen_t = (row_at <= lane_at if d == 0 else row_at >= lane_at).astype(bf16)
        cumul_rows = dot_parts(parts, seen_t)
        cumul_cols = dot_parts([seen.astype(bf16)], parts[0], ((1,), (1,)))
        for part in parts[1:]:
            cumul_cols = cumul_cols + dot(seen.astype(bf16), part, ((1,), (1,)))

        first = iota((HEAD_DIM, LANES), 1) < HEAD_DIM
        block = jnp.concatenate(
            [jnp.where(first, memory, 0.0), jnp.where(first, 0.0, memory)], axis=0
        )
        carried_out = sum(dot(query, part) for part in three_parts(block))
        carried_den = head_sums(query32 * normal, wide)

        numer, denom, carry = [], [], []
        for h in range(2):
            r = 2 * d + h
            at_query = cumul_cols[:, r : r + 1]
            spread = at_query + (rate[r : r + 1] - cumul_rows[r : r + 1])
            spread = jnp.where(seen, spread, -jnp.inf)
            carried = at_query + top_in[:, HEAD_DIM * h : HEAD_DIM * h + 1]
            row_top = jnp.maximum(carried, jnp.max(spread, axis=1, keepdims=True))
            weighted = scores[h] * jnp.exp(spread - row_top)
            carry_weight = jnp.exp(carried - row_top)
            numer.append(dot_parts(three_parts(weighted), value))
            total = jnp.sum(weighted, axis=1, keepdims=True) + carry_weight * carried_den[h]
            denom.append(jnp.maximum(jnp.abs(total), jnp.exp(-row_top)))
            carry.append(carry_weight)
        top_part = by_head(numer[0], numer[1], wide)
        top_part = top_part + by_head(carry[0], carry[1], wide) * carried_out
        summed = summed + top_part / by_head(denom[0], denom[1], wide)
    squares = head_sums(summed * summed, wide)
    mean = by_head(squares[0], squares[1], wide) * (1.0 / HEAD_DIM)
    mixed = (summed * lax.rsqrt(mean + EPS) * gain_ref[...]).astype(bf16)
    out_ref[...] = dot(mixed, exit_ref[...]).astype(bf16)


def norm_kernel(pieces_ref, skip_ref, gain_ref, middle_ref, normed_ref):
    total = skip_ref[...].astype(f32)
    projected = pieces_ref[0].astype(f32)
    for j in range(1, pieces_ref.shape[0]):
        projected = projected + pieces_ref[j].astype(f32)
    middle = (total + projected).astype(bf16)
    middle_ref[...] = middle
    wide = middle.astype(f32)
    mean = jnp.mean(wide * wide, axis=1, keepdims=True)
    normed = (wide * lax.rsqrt(mean + EPS) * gain_ref[...]).astype(bf16)
    for copy in range(normed_ref.shape[0]):
        normed_ref[copy] = normed


def pack_kernel(up_ref, gate_ref, down_ref, out_ref):
    rest = HIDDEN - MAIN
    out_ref[:, :MAIN] = up_ref[:, :MAIN]
    tails = [up_ref[:, MAIN:].astype(f32), gate_ref[:, MAIN:].astype(f32)]
    out_ref[:, MAIN:GATE_AT] = jnp.concatenate(tails, axis=1).astype(bf16)
    out_ref[:, GATE_AT:DOWN_AT] = gate_ref[:, :MAIN]
    out_ref[:, DOWN_AT : DOWN_AT + MAIN] = down_ref[:, :MAIN]
    tails = [down_ref[:, MAIN:].astype(f32), jnp.zeros((out_ref.shape[0], rest), f32)]
    out_ref[:, DOWN_AT + MAIN :] = jnp.concatenate(tails, axis=1).astype(bf16)


def gated(inner, gate, taps):
    length = gate.shape[0]
    at = iota(gate.shape, 0)
    main = inner[:length]
    after_edge = inner[length : length + 1]
    before_edge = inner[length + 1 : length + 2]
    earlier = jnp.where(at == 0, before_edge, pltpu.roll(main, 1, 0))
    later = jnp.where(at == length - 1, after_edge, pltpu.roll(main, length - 1, 0))
    conv = taps[0:1] * earlier + taps[1:2] * main + taps[2:3] * later
    return jax.nn.gelu(conv) * gate


def feed_kernel(
    core_ref,
    tokens_ref,
    edges_ref,
    weight_ref,
    taps_ref,
    own_ref,
    other_ref,
    rows_ref,
    loaded_ref,
    hidden_ref,
    sems,
):
    length, width = tokens_ref.shape
    pairs, own, _ = own_ref.shape

    def keep(hidden, cols):
        for x in range(pairs):
            for c in range(2):
                slot = core_ref[0] if c == 0 else 1 - core_ref[0]
                at = pl.multiple_of(slot * (pairs * own) + x * own, own)
                row = (2 * x + c) * own
                hidden_ref[pl.ds(at, own), cols] = hidden[row : row + own].astype(bf16)

    step = width // FEED_STEPS
    copies = []
    for i in range(FEED_STEPS + 1):
        place = (pl.ds(i * step, step), pl.ds(0, DOWN_AT))
        if i == FEED_STEPS:
            place = (pl.ds(0, width), pl.ds(DOWN_AT, PACKED - DOWN_AT))
        copies.append(
            pltpu.make_async_copy(weight_ref.at[place], loaded_ref.at[place], sems.at[i])
        )
        copies[i].start()
    rows_ref[:length, :] = tokens_ref[...]
    rows_ref[length:, :] = edges_ref[...]
    inner, gate = None, None
    for i in range(FEED_STEPS):
        copies[i].wait()
        rows = slice(i * step, (i + 1) * step)
        left = rows_ref[:, rows]
        first = dot(left, loaded_ref[rows, :GATE_AT])
        second = dot(left[:length], loaded_ref[rows, GATE_AT:DOWN_AT])
        inner = first if inner is None else inner + first
        gate = second if gate is None else gate + second
    rounded = inner.astype(bf16).astype(f32)
    hidden = gated(rounded[:, :MAIN], gate, taps_ref[:, :MAIN])
    keep(hidden, slice(0, MAIN))
    gate = pltpu.roll(inner[:length, MAIN:], 64, 1)
    hidden = gated(rounded[:, MAIN:], gate, taps_ref[:, MAIN:])
    hidden = jnp.where(iota(hidden.shape, 1) < HIDDEN - MAIN, hidden, 0.0)
    keep(hidden, slice(MAIN, None))
    copies[FEED_STEPS].wait()
    for at in range(0, width, 256):
        cols = slice(at, at + 256)
        part = dot(hidden_ref[...], loaded_ref[cols, DOWN_AT:], ((1,), (1,))).astype(bf16)
        own_ref[:, :, cols] = part[: length // 2].reshape(pairs, own, 256)
        other_ref[:, :, cols] = part[length // 2 :].reshape(pairs, own, 256)


def near(x):
    return pltpu.with_memory_space_constraint(x, pltpu.VMEM)


def whole_call(kernel, out_shape, in_specs, name):
    def call(*args):
        return pl.pallas_call(
            kernel,
            out_shape=out_shape,
            in_specs=in_specs,
            out_specs=jax.tree.map(lambda _: VMEM, out_shape),
            name=name,
        )(*args)

    return call


def shape_of(dims, dtype):
    return jax.ShapeDtypeStruct(dims, dtype)


def exchanged(pieces, axis):
    return lax.all_to_all(pieces, axis, split_axis=0, concat_axis=0, tiled=True)


def body(
    lookup_request_vectors,
    lookup_address_vectors,
    lookup_content_vectors,
    admission_preactivation,
    retention_preactivation,
    extra_decay_terms,
    per_slot_rescale_factor,
    mixer_exit_matrix,
    skip_path_activity,
    mlp_rescale_factor,
    filter_widening_matrix,
    multiplier_widening_matrix,
    neighbour_filter_coefficients,
    contracting_matrix,
):
    length = lookup_request_vectors.shape[0]
    width = mixer_exit_matrix.shape[1]
    members = lax.axis_size(TP)

    packed = whole_call(
        pack_kernel, shape_of((filter_widening_matrix.shape[0], PACKED), bf16), [VMEM] * 3, "pack"
    )(filter_widening_matrix, multiplier_widening_matrix, contracting_matrix.T)
    weights = lax.all_gather(packed, SP, axis=0, tiled=True)

    decay = jax.nn.log_sigmoid(retention_preactivation) + extra_decay_terms
    rate = admission_preactivation

    state = pltpu.VMEM((8, STATE_ROWS, LANES), f32)
    summary = whole_call(summarize_kernel, state, [VMEM] * 4, "summarize")(
        lookup_address_vectors, lookup_content_vectors, rate, decay
    )
    pieces = near(exchanged(summary, "sp_1"))
    along, inside, inside_tail = whole_call(
        combine_kernel,
        (
            pltpu.VMEM((8, HALF_ROWS, LANES), f32),
            pltpu.VMEM((128, LANES), f32),
            pltpu.VMEM((8, LANES), f32),
        ),
        [SMEM, VMEM],
        "combine",
    )(jnp.stack([lax.axis_index("sp_1"), lax.axis_index("sp_0")]), pieces)
    pieces = near(exchanged(along, "sp_0"))
    partial_out = whole_call(
        mix_kernel, pltpu.VMEM((length, width), bf16), [SMEM] + [VMEM] * 10, "mix"
    )(
        lax.axis_index("sp_0").reshape(1),
        pieces,
        near(inside),
        near(inside_tail),
        lookup_request_vectors,
        lookup_address_vectors,
        lookup_content_vectors,
        rate,
        decay,
        per_slot_rescale_factor.reshape(1, LANES),
        mixer_exit_matrix,
    )
    own = length // members
    pieces = near(exchanged(partial_out.reshape(members, own, width), TP))
    middle, normed = whole_call(
        norm_kernel,
        (shape_of((own, width), bf16), pltpu.VMEM((members, own, width), bf16)),
        [VMEM] * 3,
        "norm",
    )(pieces, skip_path_activity, mlp_rescale_factor.reshape(1, width))
    tokens = exchanged(normed, TP).reshape(length, width)

    peers = lax.axis_size(SP)
    up = [(i, i + 1) for i in range(peers - 1)]
    down = [(j, i) for i, j in up]
    earlier = lax.ppermute(tokens[length - 1 :], SP, up)
    later = lax.ppermute(tokens[:1], SP, down)
    edges = jnp.concatenate([later, earlier, jnp.zeros((14, width), bf16)], axis=0)

    halves = pltpu.VMEM((members // 2, own, width), bf16)
    own_half, other_half = pl.pallas_call(
        feed_kernel,
        out_shape=(halves, halves),
        in_specs=[SMEM, VMEM, VMEM, ANY, VMEM],
        out_specs=(VMEM, VMEM),
        scratch_shapes=[
            pltpu.VMEM((length + 16, width), bf16),
            pltpu.VMEM((width, PACKED), bf16),
            pltpu.VMEM((length, 768), bf16),
            pltpu.SemaphoreType.DMA((FEED_STEPS + 1,)),
        ],
        name="feed",
    )(
        lax.axis_index("core").reshape(1),
        near(tokens),
        near(edges),
        pltpu.with_memory_space_constraint(weights, pltpu.HBM),
        jnp.pad(neighbour_filter_coefficients, ((0, 0), (0, 768 - HIDDEN))),
    )
    from_partner = lax.ppermute(other_half, "core", [(0, 1), (1, 0)])
    pair = (own_half.astype(f32) + from_partner.astype(f32)).astype(bf16)
    pieces = exchanged(pair, "x").astype(f32)
    total = middle.astype(f32)
    for j in range(pieces.shape[0]):
        total = total + pieces[j]
    return total.astype(bf16)


def solution(mesh):
    split = Mesh(mesh.devices.reshape(8, 8, 4, 2), SP_TP)
    placed = (
        P(SP, TP),
        P(SP, TP),
        P(SP, TP),
        P(None, TP, SP),
        P(None, TP, SP),
        P(None, TP, SP),
        P(TP),
        P(TP, None),
        P(SP_TP, None),
        P(),
        P(SP, TP),
        P(SP, TP),
        P(None, TP),
        P(TP, SP),
    )
    return jax.shard_map(
        body, mesh=split, in_specs=placed, out_specs=P(SP_TP, None), check_vma=False
    )
```

time: 270 us -> 152 us (0.56)
  blocking collectives: 164 us -> 78.9 us
  local copies, waits for them, and re-layouts: 32.9 us -> 0.71 us
  matrix products: 21.5 us -> 0 us
  Pallas kernels: 0 us -> 16.6 us
  other arithmetic: 18.1 us -> 3.01 us
  starting transfers between devices: 4.38 us -> 15.7 us
  waiting for transfers between devices: 12.9 us -> 22.5 us
    all_gather x4 -> x0, blocking collectives: 92.2 us -> none  [gathered_once(): both, at, found = (lax.all_gather(jnp.concatenate(lines), axis), 0, {})]
    dot_general x31 -> x0, matrix products: 21.5 us -> none  [the longest x1 7.85 us: body(): jnp.dot(hidden, whole_down, preferred_element_type=jnp.float32)]
    pallas_call x0 -> x6, Pallas kernels: none -> 16.6 us  [the longest x5 10.5 us: call(): pl.pallas_call(kernel, out_shape=out_shape, in_specs=in_specs, out_specs=...]
    all_to_all x0 -> x1, waiting for transfers between devices: none -> 15.1 us  [exchanged(): return lax.all_to_all(pieces, axis, split_axis=0, concat_axis=0, tiled=True)]
    slice x53 -> x1, local copies, waits for them, and re-layouts: 11.6 us -> 0.02 us  [body(): later = lax.ppermute(tokens[:1], SP, down)]
    ppermute x2 -> x3, waiting for transfers between devices: 9.42 us -> 1.59 us  [the longest x1 1.51 us: body(): from_partner = lax.ppermute(other_half, 'core', [(0, 1), (1, 0)])]
    all_to_all x0 -> x1, starting transfers between devices: none -> 7.64 us  [exchanged(): return lax.all_to_all(pieces, axis, split_axis=0, concat_axis=0, tiled=True)]
    all_to_all x3 -> x4, blocking collectives: 71.5 us -> 78.9 us  [exchanged(): return lax.all_to_all(pieces, axis, split_axis=0, concat_axis=0, tiled=True)]
  transfers between devices with their start and end apart: 5 -> 5, of which waited for: 3 -> 4; matrix products, arithmetic and copies ran while one was open for 23% -> 2% of each run, Pallas kernels for 0% -> 6%
where the time goes in v1:
time: 152 us; the launch traced here: 151 us
  blocking collectives  78.9 us (52%)
  waiting for transfers between devices  22.5 us (15%)
  Pallas kernels  16.6 us (11%)
  starting transfers between devices  15.7 us (10%)
  between operations  13.5 us (9%)
  other arithmetic  3.01 us (2%)
    all_to_all x4, blocking collectives, exchanged(): return lax.all_to_all(pieces, axis, split_axis=0, concat_axis=0, tiled=True)  78.9 us
    all_to_all x1, waiting for transfers between devices, exchanged(): return lax.all_to_all(pieces, axis, split_axis=0, concat_axis=0, tiled=True)  15.1 us
    pallas_call x5, Pallas kernels, call(): pl.pallas_call(kernel, out_shape=out_shape, in_specs=in_specs, out_specs=...  10.5 us
    all_to_all x1, starting transfers between devices, exchanged(): return lax.all_to_all(pieces, axis, split_axis=0, concat_axis=0, tiled=True)  7.64 us
    pallas_call x1, Pallas kernels, body(): pl.pallas_call(feed_kernel, out_shape=(halves, halves), in_specs=[SMEM, V...  6.06 us
    all_gather x1, waiting for transfers between devices, body(): weights = lax.all_gather(packed, SP, axis=0, tiled=True)  5.73 us
    ppermute x1, starting transfers between devices, body(): earlier = lax.ppermute(tokens[length - 1:], SP, up)  3.99 us
  transfers between devices with their start and end apart: 5, of which 4 were waited for; matrix products, arithmetic and copies ran while one was open for 2% of the time, Pallas kernels for 6%

profile of v1, /device:TPU:1, one launch (start us, length us, event | category | flops | bytes accessed | tf_op | source)
XLA Modules:
  0.0 150.8 jit_solution(6237021664324142498)
XLA Ops:
  6.5 0.0 copy-start.1
  6.5 0.0 all-gather.2.cloned.1.call-start
  6.5 1.6 %pack.1 = bf16[32,2176]{1,0:T(8,128)(2,1)} custom-call(bf16[32,704]{1,0:T(8,128)(2,1)} %up_ref.1, bf16[32,704]{1,0:T(8,128)(2,1)} %gate_ref.1, bf16[32,704]{1,0:T(8,128)(2,1)} %bitcast.35), custom_call_target="tpu_custom_call" | custom-call | tf_op jit(solution)/shard_map/pack/pallas_call | solution.py:381
  8.1 0.0 all-gather.2.cloned.1.call-update
  8.2 1.3 fusion.6.decay_ref
  9.5 2.4 %summarize.1 = f32[8,136,128]{2,1,0:T(8,128)} custom-call(bf16[256,128]{1,0:T(8,128)(2,1)} %key_ref.3, bf16[256,128]{1,0:T(8,128)(2,1)} %value_ref.3, f32[2,2,256]{2,1,0:T(2,128)} %rate_ref.3, f32[2,2,256]{2,1,0:T(2,128)} %fusion.6.decay_ref), custom_call_target="tpu_custom_call" | custom-call | tf_op jit(solution)/shard_map/summarize/pallas_call | solution.py:381
  11.9 7.6 %all-to-all-start = ((f32[8,136,128]{2,1,0:T(8,128)}), f32[8,136,128]{2,1,0:T(8,128)S(1)}, u32[]{:S(2)}, u32[]{:S(2)}) async-start(f32[8,136,128]{2,1,0:T(8,128)} %summarize.1), calls=%async_computation | async-start | bytes 1114112 | tf_op jit(solution)/shard_map/all_to_all | solution.py:397
  19.5 0.7 pad_add_fusion.here_ref
  20.2 15.1 %all-to-all-done.pieces_ref = f32[8,136,128]{2,1,0:T(8,128)S(1)} async-done(((f32[8,136,128]{2,1,0:T(8,128)}), f32[8,136,128]{2,1,0:T(8,128)S(1)}, u32[]{:S(2)}, u32[]{:S(2)}) %all-to-all-start) | async-done | bytes 557088 | tf_op jit(solution)/shard_map/all_to_all | solution.py:397
  35.3 0.8 combine.1
  36.1 28.0 %all_to_all.25.pieces_ref = f32[8,72,128]{2,1,0:T(8,128)S(1)} all-to-all(f32[8,72,128]{2,1,0:T(8,128)S(1)} %get-tuple-element.12), channel_id=1, replica_groups=mesh['sp_0'=8,'sp_1'=8,'x'=4,'core'=2] {'sp_0'}, dimensions={0} | all-to-all | bytes 589824 | tf_op jit(solution)/shard_map/all_to_all | solution.py:397
  64.1 4.0 %mix.1 = bf16[256,2048]{1,0:T(8,128)(2,1)S(1)} custom-call(s32[1]{0:T(128)} %bitcast.here_ref, f32[8,72,128]{2,1,0:T(8,128)S(1)} %all_to_all.25.pieces_ref, f32[128,128]{1,0:T(8,128)S(1)} %get-tuple-element.13.inside_ref, f32[8,128]{1,0:T(8,128)S(1)} %get-tuple-element.14.inside_tail_ref, bf16[256,128]{1,0:T(8,128)(2,1)} %query_ref.1, ...), custom_call_target="tpu_custom_call" | custom-call | tf_op jit(solution)/shard_map/mix/pallas_call | solution.py:381
  68.1 20.0 %all_to_all.26.pieces_ref = bf16[8,32,2048]{2,1,0:T(8,128)(2,1)S(1)} all-to-all(bf16[8,32,2048]{2,1,0:T(8,128)(2,1)S(1)} %bitcast.34), channel_id=1, replica_groups=mesh['sp_0'=8,'sp_1'=8,'x'=4,'core'=2] {'x','core'}, dimensions={0} | all-to-all | bytes 2097152 | tf_op jit(solution)/shard_map/all_to_all | solution.py:397
  88.1 1.7 %norm.1 = (bf16[32,2048]{1,0:T(8,128)(2,1)}, bf16[8,32,2048]{2,1,0:T(8,128)(2,1)S(1)}) custom-call(bf16[8,32,2048]{2,1,0:T(8,128)(2,1)S(1)} %all_to_all.26.pieces_ref, bf16[32,2048]{1,0:T(8,128)(2,1)} %skip_ref.1, f32[1,2048]{1,0:T(1,128)} %bitcast.36), custom_call_target="tpu_custom_call" | custom-call | tf_op jit(solution)/shard_map/norm/pallas_call | solution.py:381
  89.9 0.0 copy-start
  89.9 18.5 %all_to_all.27 = bf16[8,32,2048]{2,1,0:T(8,128)(2,1)S(1)} all-to-all(bf16[8,32,2048]{2,1,0:T(8,128)(2,1)S(1)} %get-tuple-element.16), channel_id=1, replica_groups=mesh['sp_0'=8,'sp_1'=8,'x'=4,'core'=2] {'x','core'}, dimensions={0} | all-to-all | bytes 2097152 | tf_op jit(solution)/shard_map/all_to_all | solution.py:397
  108.4 1.3 collective-permute-start
  109.7 4.0 %collective-permute-start.1 = (bf16[1,2048]{1,0:T(2,128)(2,1)S(1)}, bf16[1,2048]{1,0:T(2,128)(2,1)S(1)}, u32[]{:S(2)}, u32[]{:S(2)}) collective-permute-start(bf16[1,2048]{1,0:T(2,128)(2,1)S(1)} %get-tuple-element.20), channel_id=1, source_target_pairs={{0,8},{8,16},{16,24},{24,32},{32,40},{40,48},{48,56},{56,64},{64,7... | collective-permute-start | bytes 12296 | tf_op jit(solution)/shard_map/ppermute | solution.py:472
  113.7 0.1 pad.7.clone
  113.8 0.0 copy-done.1
  113.8 0.6 pad.4.taps_ref
  114.4 0.0 collective-permute-done
  114.4 0.1 collective-permute-done.1
  114.5 0.1 maximum_maximum_fusion.edges_ref
  114.5 5.7 %all-gather.2.cloned.1.call-done.weight_ref = bf16[2048,2176]{1,0:T(8,128)(2,1)} async-done(((bf16[32,2176]{1,0:T(8,128)(2,1)}), bf16[2048,2176]{1,0:T(8,128)(2,1)}) %all-gather.2.cloned.1.call-update) | async-done | bytes 8912912 | tf_op jit(solution)/shard_map/all_gather | solution.py:423
  120.3 6.1 %feed.1 = (bf16[4,32,2048]{2,1,0:T(8,128)(2,1)S(1)}, bf16[4,32,2048]{2,1,0:T(8,128)(2,1)S(1)}) custom-call(s32[1]{0:T(128)} %bitcast.5.core_ref, bf16[256,2048]{1,0:T(8,128)(2,1)S(1)} %bitcast.33, bf16[16,2048]{1,0:T(8,128)(2,1)S(1)} %maximum_maximum_fusion.edges_ref, bf16[2048,2176]{1,0:T(8,128)(2,1)} %all-gather.2.cloned.1.call-done.weight_ref, ...), custom_call_target="tpu_custom_call" | custom-call | tf_op jit(solution)/shard_map/feed/pallas_call | solution.py:477
  126.3 2.7 %collective-permute-start.2 = (bf16[4,32,2048]{2,1,0:T(8,128)(2,1)S(1)}, bf16[4,32,2048]{2,1,0:T(8,128)(2,1)S(1)}, u32[]{:S(2)}, u32[]{:S(2)}) collective-permute-start(bf16[4,32,2048]{2,1,0:T(8,128)(2,1)S(1)} %get-tuple-element.18), channel_id=1, source_target_pairs={{0,1},{1,0},{2,3},{3,2},{4,5},{5,4},{6,7},{7,6},{8,9},{9,8},{10,11... | collective-permute-start | bytes 1572872 | tf_op jit(solution)/shard_map/ppermute | solution.py:496
  129.1 1.5 %collective-permute-done.2 = bf16[4,32,2048]{2,1,0:T(8,128)(2,1)S(1)} collective-permute-done((bf16[4,32,2048]{2,1,0:T(8,128)(2,1)S(1)}, bf16[4,32,2048]{2,1,0:T(8,128)(2,1)S(1)}, u32[]{:S(2)}, u32[]{:S(2)}) %collective-permute-start.2) | collective-permute-done | bytes 524320 | tf_op jit(solution)/shard_map/ppermute | solution.py:496
  130.6 0.1 add_convert_fusion
  130.7 12.4 %all_to_all.28 = bf16[4,32,2048]{2,1,0:T(8,128)(2,1)S(1)} all-to-all(bf16[4,32,2048]{2,1,0:T(8,128)(2,1)S(1)} %add_convert_fusion), channel_id=1, replica_groups=mesh['sp_0'=8,'sp_1'=8,'x'=4,'core'=2] {'x'}, dimensions={0} | all-to-all | bytes 1048576 | tf_op jit(solution)/shard_map/all_to_all | solution.py:397
  143.1 0.1 convert_element_type.24
  143.2 0.0 copy-done
  143.2 0.7 fusion.1
  (2 shorter events, 0.0 us)
Async XLA Ops:
  6.5 107.2 %copy-start.1 = (f32[3,704]{1,0:T(4,128)S(1)}, f32[3,704]{1,0:T(4,128)}, u32[]{:S(2)}) copy-start(f32[3,704]{1,0:T(4,128)} %param.26) | copy-start | bytes 25348
  6.5 113.7 %all-gather.2.cloned.1.call-start = ((), (), s32[]{:S(2)}) async-start(), calls=%async_computation.5 | async-start | bytes 9052160 | tf_op jit(solution)/shard_map/all_gather | solution.py:423
  11.9 23.4 %all-to-all-start = ((f32[8,136,128]{2,1,0:T(8,128)}), f32[8,136,128]{2,1,0:T(8,128)S(1)}, u32[]{:S(2)}, u32[]{:S(2)}) async-start(f32[8,136,128]{2,1,0:T(8,128)} %summarize.1), calls=%async_computation | async-start | bytes 1114112 | tf_op jit(solution)/shard_map/all_to_all | solution.py:397
  89.9 53.4 %copy-start = (bf16[32,2048]{1,0:T(8,128)(2,1)S(1)}, bf16[32,2048]{1,0:T(8,128)(2,1)}, u32[]{:S(2)}) copy-start(bf16[32,2048]{1,0:T(8,128)(2,1)} %get-tuple-element.15) | copy-start | bytes 393220
  108.4 6.0 %collective-permute-start = (bf16[1,2048]{1,0:T(2,128)(2,1)S(1)}, bf16[1,2048]{1,0:T(2,128)(2,1)S(1)}, u32[]{:S(2)}, u32[]{:S(2)}) collective-permute-start(bf16[1,2048]{1,0:T(2,128)(2,1)S(1)} %get-tuple-element.19), channel_id=1, source_target_pairs={{8,0},{16,8},{24,16},{32,24},{40,32},{48,40},{56,48},{64,56},{72,6... | collective-permute-start | bytes 12296 | tf_op jit(solution)/shard_map/ppermute | solution.py:473
  109.7 4.8 %collective-permute-start.1 = (bf16[1,2048]{1,0:T(2,128)(2,1)S(1)}, bf16[1,2048]{1,0:T(2,128)(2,1)S(1)}, u32[]{:S(2)}, u32[]{:S(2)}) collective-permute-start(bf16[1,2048]{1,0:T(2,128)(2,1)S(1)} %get-tuple-element.20), channel_id=1, source_target_pairs={{0,8},{8,16},{16,24},{24,32},{32,40},{40,48},{48,56},{56,64},{64,7... | collective-permute-start | bytes 12296 | tf_op jit(solution)/shard_map/ppermute | solution.py:472
  126.3 4.3 %collective-permute-start.2 = (bf16[4,32,2048]{2,1,0:T(8,128)(2,1)S(1)}, bf16[4,32,2048]{2,1,0:T(8,128)(2,1)S(1)}, u32[]{:S(2)}, u32[]{:S(2)}) collective-permute-start(bf16[4,32,2048]{2,1,0:T(8,128)(2,1)S(1)} %get-tuple-element.18), channel_id=1, source_target_pairs={{0,1},{1,0},{2,3},{3,2},{4,5},{5,4},{6,7},{7,6},{8,9},{9,8},{10,11... | collective-permute-start | bytes 1572872 | tf_op jit(solution)/shard_map/ppermute | solution.py:496
Sparse Core Ops, SparseCore 0:
  10.3 109.8 all-gather.1

commit v2 on v1

--- a/solution.py
+++ b/solution.py
@@ -12,8 +12,6 @@
 SP_TP = SP + TP
 EPS = 1e-06
 FAR_BELOW = -1e30
-STATE_ROWS = 136
-HALF_ROWS = 72
 LANES = 128
 HIDDEN = 704
 MAIN = 640
@@ -64,36 +62,31 @@
     return jnp.where(iota(shape, len(shape) - 1) < HEAD_DIM, first, second)
 
 
-def packed_tail(rows):
-    place = iota((8, LANES), 0)
-    out = jnp.zeros((8, LANES), f32)
+def packed_rows(rows, count):
+    place = iota((count, LANES), 0)
+    out = jnp.zeros((count, LANES), f32)
     for k, row in enumerate(rows):
         out = jnp.where(place == k, row, out)
     return out
 
 
-def write_state(out_ref, memories, normals, totals, tops):
-    tail = packed_tail([*normals, *totals, *tops])
-    for copy in range(out_ref.shape[0]):
-        for d in range(2):
-            out_ref[copy, 64 * d : 64 * (d + 1), :] = memories[d]
-        out_ref[copy, 128:, :] = tail
-
-
-def write_halves(out_ref, here, memories, normals, totals, tops):
-    tails = [packed_tail([normals[d], totals[d], tops[d]]) for d in range(2)]
-    for copy in range(out_ref.shape[0]):
-        later = copy > here
-        out_ref[copy, :64, :] = jnp.where(later, memories[0], memories[1])
-        out_ref[copy, 64:, :] = jnp.where(later, tails[0], tails[1])
-
-
-def read_state(ref, j, d):
-    if ref.shape[1] == HALF_ROWS:
-        tail, at, step = ref[j, 64:, :], 0, 1
-    else:
-        tail, at, step = ref[j, 128:, :], d, 2
-    return tuple(tail[at + k * step : at + k * step + 1] for k in range(3))
+def nothing(rows):
+    line = jnp.zeros((1, LANES), f32)
+    return line, jnp.zeros((rows, LANES), f32), line, jnp.full((1, LANES), FAR_BELOW, f32)
+
+
+def combined(earlier, later):
+    total_a, memory_a, normal_a, top_a = earlier
+    total_b, memory_b, normal_b, top_b = later
+    lifted = total_b + top_a
+    top = jnp.maximum(lifted, top_b)
+    weight_a, weight_b = jnp.exp(lifted - top), jnp.exp(top_b - top)
+    memory = weight_a * memory_a + weight_b * memory_b
+    return total_a + total_b, memory, weight_a * normal_a + weight_b * normal_b, top
+
+
+def in_order(d, peers):
+    return range(peers) if d == 0 else reversed(range(peers))
 
 
 def summarize_kernel(key_ref, value_ref, rate_ref, decay_ref, out_ref):
@@ -126,64 +119,65 @@
         normals.append(by_head(normal_all[a : a + 1], normal_all[b : b + 1], row))
         totals.append(by_head(total[a : a + 1], total[b : b + 1], row))
         tops.append(by_head(top[a : a + 1], top[b : b + 1], row))
-    write_state(out_ref, memories, normals, totals, tops)
-
-
-def weigh(entries, order, active):
-    row = (1, LANES)
-    since = jnp.zeros(row, f32)
-    exponents = {}
-    for j in order:
-        _, total, top = entries[j]
-        on = active(j)
-        exponents[j] = jnp.where(on, top + since, FAR_BELOW)
-        since = since + jnp.where(on, total, 0.0)
-    highest = jnp.full(row, FAR_BELOW, f32)
-    for j in order:
-        highest = jnp.maximum(highest, exponents[j])
-    weights = {
-        j: jnp.where(active(j), jnp.exp(exponents[j] - highest), 0.0) for j in order
-    }
-    return weights, since, highest
-
-
-def gathered(ref, entries, weights, d):
-    memory = jnp.zeros((HEAD_DIM, LANES), f32)
-    normal = jnp.zeros((1, LANES), f32)
-    for j, w in weights.items():
-        at = 0 if ref.shape[1] == HALF_ROWS else 64 * d
-        memory = memory + w * ref[j, at : at + 64, :]
-        normal = normal + w * entries[j][0]
-    return memory, normal
-
-
-def nearest_first(d, peers):
-    return list(reversed(range(peers))) if d == 0 else list(range(peers))
-
-
-def before(d, here):
-    return (lambda j: j < here) if d == 0 else (lambda j: j > here)
-
-
-def combine_kernel(here_ref, pieces_ref, out_ref, inside_ref, inside_tail_ref):
+    tail = packed_rows([*normals, *totals, *tops], 8)
+    for j in range(out_ref.shape[0]):
+        part = [memory[8 * j : 8 * (j + 1)] for memory in memories]
+        out_ref[j, :16, :] = jnp.concatenate(part, axis=0)
+        out_ref[j, 16:, :] = tail
+
+
+def along_kernel(here_ref, pieces_ref, out_ref, inside_ref):
+    peers = pieces_ref.shape[0]
+    tails = [pieces_ref[j, 16:, :] for j in range(peers)]
+    memories = [pieces_ref[j, :16, :] for j in range(peers)]
+    reaching = []
+    wholes = []
+    for d in range(2):
+        state = nothing(8)
+        reached = {}
+        for j in in_order(d, peers):
+            reached[j] = state
+            normal, total, top = (tails[j][d + k : d + k + 1] for k in (0, 2, 4))
+            state = combined(state, (total, memories[j][8 * d : 8 * (d + 1)], normal, top))
+        reaching.append(reached)
+        total, memory, normal, top = state
+        rows = packed_rows([normal, total, top], 8)
+        wholes.append(jnp.concatenate([memory, rows], axis=0))
+    for j in range(peers):
+        lines = []
+        for d in range(2):
+            total, memory, normal, top = reaching[d][j]
+            inside_ref[j, 8 * d : 8 * (d + 1), :] = memory
+            lines += [total, normal, top]
+        inside_ref[j, 16:, :] = packed_rows(lines, 8)
+    for j in range(out_ref.shape[0]):
+        out_ref[j] = jnp.where(j > here_ref[0], wholes[0], wholes[1])
+
+
+def across_kernel(here_ref, pieces_ref, inside_ref, out_ref):
     peers = pieces_ref.shape[0]
     here = here_ref[0]
-    memories, normals, totals, tops, tail = [], [], [], [], []
+    far = []
     for d in range(2):
-        entries = [read_state(pieces_ref, j, d) for j in range(peers)]
-        order = nearest_first(d, peers)
-        weights, since, highest = weigh(entries, order, before(d, here))
-        memory, normal = gathered(pieces_ref, entries, weights, d)
-        inside_ref[64 * d : 64 * (d + 1), :] = memory
-        tail += [normal, since, highest]
-        weights, since, highest = weigh(entries, order, lambda j: j >= 0)
-        memory, normal = gathered(pieces_ref, entries, weights, d)
-        memories.append(memory)
-        normals.append(normal)
-        totals.append(since)
-        tops.append(highest)
-    inside_tail_ref[...] = packed_tail(tail)
-    write_halves(out_ref, here_ref[1], memories, normals, totals, tops)
+        state = nothing(8)
+        for j in in_order(d, peers):
+            piece = pieces_ref[j]
+            later = (piece[9:10], piece[:8], piece[8:9], piece[10:11])
+            on = j < here if d == 0 else j > here
+            state = [jnp.where(on, x, y) for x, y in zip(combined(state, later), state)]
+        far.append(state)
+    for j in range(out_ref.shape[0]):
+        memories, normals, tops = [], [], []
+        lines = inside_ref[j, 16:, :]
+        for d in range(2):
+            total, normal, top = (lines[3 * d + k : 3 * d + k + 1] for k in range(3))
+            near_state = (total, inside_ref[j, 8 * d : 8 * (d + 1), :], normal, top)
+            _, memory, normal, top = combined(far[d], near_state)
+            memories.append(memory)
+            normals.append(normal)
+            tops.append(top)
+        out_ref[j, :16, :] = jnp.concatenate(memories, axis=0)
+        out_ref[j, 16:, :] = packed_rows(normals + tops, 8)
 
 
 def head_sums(x, shape):
@@ -194,10 +188,7 @@
 
 
 def mix_kernel(
-    here_ref,
     pieces_ref,
-    inside_ref,
-    inside_tail_ref,
     query_ref,
     key_ref,
     value_ref,
@@ -208,7 +199,7 @@
     out_ref,
 ):
     peers = pieces_ref.shape[0]
-    here = here_ref[0]
+    tail = pieces_ref[0, 16:, :]
     length = query_ref.shape[0]
     wide = (length, LANES)
     query = query_ref[...]
@@ -225,18 +216,10 @@
         scores.append(dot(own, key_ref[...], ((1,), (1,))) * HEAD_DIM ** (-0.5))
     summed = jnp.zeros(wide, f32)
     for d in range(2):
-        entries = [read_state(pieces_ref, j, d) for j in range(peers)]
-        weights, _, far_top = weigh(entries, nearest_first(d, peers), before(d, here))
-        far_memory, far_normal = gathered(pieces_ref, entries, weights, d)
-        near_normal = inside_tail_ref[3 * d : 3 * d + 1]
-        near_total = inside_tail_ref[3 * d + 1 : 3 * d + 2]
-        near_top = inside_tail_ref[3 * d + 2 : 3 * d + 3]
-        lifted = near_total + far_top
-        top_in = jnp.maximum(lifted, near_top)
-        far_weight = jnp.exp(lifted - top_in)
-        near_weight = jnp.exp(near_top - top_in)
-        memory = far_weight * far_memory + near_weight * inside_ref[64 * d : 64 * (d + 1), :]
-        normal = far_weight * far_normal + near_weight * near_normal
+        memory = jnp.concatenate(
+            [pieces_ref[j, 8 * d : 8 * (d + 1), :] for j in range(peers)], axis=0
+        )
+        normal, top_in = tail[d : d + 1], tail[2 + d : 3 + d]
 
         seen = row_at >= lane_at if d == 0 else row_at <= lane_at
         seen_t = (row_at <= lane_at if d == 0 else row_at >= lane_at).astype(bf16)
@@ -425,29 +408,24 @@
     decay = jax.nn.log_sigmoid(retention_preactivation) + extra_decay_terms
     rate = admission_preactivation
 
-    state = pltpu.VMEM((8, STATE_ROWS, LANES), f32)
-    summary = whole_call(summarize_kernel, state, [VMEM] * 4, "summarize")(
+    row, column = lax.axis_index("sp_0").reshape(1), "sp_1"
+    pieces = pltpu.VMEM((8, 24, LANES), f32)
+    summary = whole_call(summarize_kernel, pieces, [VMEM] * 4, "summarize")(
         lookup_address_vectors, lookup_content_vectors, rate, decay
     )
-    pieces = near(exchanged(summary, "sp_1"))
-    along, inside, inside_tail = whole_call(
-        combine_kernel,
-        (
-            pltpu.VMEM((8, HALF_ROWS, LANES), f32),
-            pltpu.VMEM((128, LANES), f32),
-            pltpu.VMEM((8, LANES), f32),
-        ),
+    along, inside = whole_call(
+        along_kernel,
+        (pltpu.VMEM((8, 16, LANES), f32), pltpu.VMEM((8, 24, LANES), f32)),
         [SMEM, VMEM],
-        "combine",
-    )(jnp.stack([lax.axis_index("sp_1"), lax.axis_index("sp_0")]), pieces)
-    pieces = near(exchanged(along, "sp_0"))
+        "along",
+    )(row, near(exchanged(summary, column)))
+    across = whole_call(across_kernel, pieces, [SMEM, VMEM, VMEM], "across")(
+        row, near(exchanged(along, "sp_0")), near(inside)
+    )
     partial_out = whole_call(
-        mix_kernel, pltpu.VMEM((length, width), bf16), [SMEM] + [VMEM] * 10, "mix"
+        mix_kernel, pltpu.VMEM((length, width), bf16), [VMEM] * 8, "mix"
     )(
-        lax.axis_index("sp_0").reshape(1),
-        pieces,
-        near(inside),
-        near(inside_tail),
+        near(exchanged(across, column)),
         lookup_request_vectors,
         lookup_address_vectors,
         lookup_content_vectors,

time: 152 us -> 150 us (0.987)
  waiting for transfers between devices: 22.5 us -> 18.2 us
  blocking collectives: 78.9 us -> 82 us
    all_to_all x1, waiting for transfers between devices: 15.1 us -> 7.58 us  [exchanged(): return lax.all_to_all(pieces, axis, split_axis=0, concat_axis=0, tiled=True)]
    all_gather x1, waiting for transfers between devices: 5.73 us -> 9.11 us  [body(): weights = lax.all_gather(packed, SP, axis=0, tiled=True)]
    all_to_all x4 -> x5, blocking collectives: 78.9 us -> 82 us  [exchanged(): return lax.all_to_all(pieces, axis, split_axis=0, concat_axis=0, tiled=True)]
    pallas_call x5 -> x6, Pallas kernels: 10.5 us -> 9.63 us  [call(): pl.pallas_call(kernel, out_shape=out_shape, in_specs=in_specs, out_specs=...]
  transfers between devices with their start and end apart: 5 -> 5, of which waited for: 4 -> 3; matrix products, arithmetic and copies ran while one was open for 2% -> 2% of each run, Pallas kernels for 6% -> 5%
where the time goes in v2:
time: 150 us; the launch traced here: 149 us
  blocking collectives  82 us (55%)
  waiting for transfers between devices  18.2 us (12%)
  starting transfers between devices  15.7 us (10%)
  Pallas kernels  15.7 us (10%)
  between operations  13.5 us (9%)
  other arithmetic  2.34 us (2%)
    all_to_all x5, blocking collectives, exchanged(): return lax.all_to_all(pieces, axis, split_axis=0, concat_axis=0, tiled=True)  82 us
    pallas_call x6, Pallas kernels, call(): pl.pallas_call(kernel, out_shape=out_shape, in_specs=in_specs, out_specs=...  9.63 us
    all_gather x1, waiting for transfers between devices, body(): weights = lax.all_gather(packed, SP, axis=0, tiled=True)  9.11 us
    all_to_all x1, starting transfers between devices, exchanged(): return lax.all_to_all(pieces, axis, split_axis=0, concat_axis=0, tiled=True)  7.64 us
    all_to_all x1, waiting for transfers between devices, exchanged(): return lax.all_to_all(pieces, axis, split_axis=0, concat_axis=0, tiled=True)  7.58 us
    pallas_call x1, Pallas kernels, body(): pl.pallas_call(feed_kernel, out_shape=(halves, halves), in_specs=[SMEM, V...  6.05 us
    ppermute x1, starting transfers between devices, body(): earlier = lax.ppermute(tokens[length - 1:], SP, up)  3.99 us
  transfers between devices with their start and end apart: 5, of which 3 were waited for; matrix products, arithmetic and copies ran while one was open for 2% of the time, Pallas kernels for 5%

profile of v2, /device:TPU:1, one launch (start us, length us, event | category | flops | bytes accessed | tf_op | source)
XLA Modules:
  0.0 148.8 jit_solution(7320898434982540889)
XLA Ops:
  6.5 0.0 all-gather.2.cloned.1.call-start
  6.5 1.6 %pack.1 = bf16[32,2176]{1,0:T(8,128)(2,1)} custom-call(bf16[32,704]{1,0:T(8,128)(2,1)} %up_ref.1, bf16[32,704]{1,0:T(8,128)(2,1)} %gate_ref.1, bf16[32,704]{1,0:T(8,128)(2,1)} %bitcast.34), custom_call_target="tpu_custom_call" | custom-call | tf_op jit(solution)/shard_map/pack/pallas_call | solution.py:364
  8.1 0.0 all-gather.2.cloned.1.call-update
  8.1 1.3 fusion.6.decay_ref
  9.5 2.2 %summarize.1 = f32[8,24,128]{2,1,0:T(8,128)} custom-call(bf16[256,128]{1,0:T(8,128)(2,1)} %key_ref.3, bf16[256,128]{1,0:T(8,128)(2,1)} %value_ref.3, f32[2,2,256]{2,1,0:T(2,128)} %rate_ref.3, f32[2,2,256]{2,1,0:T(2,128)} %fusion.6.decay_ref), custom_call_target="tpu_custom_call" | custom-call | tf_op jit(solution)/shard_map/summarize/pallas_call | solution.py:364
  11.7 7.6 %all-to-all-start = ((f32[8,24,128]{2,1,0:T(8,128)}), f32[8,24,128]{2,1,0:T(8,128)S(1)}, u32[]{:S(2)}, u32[]{:S(2)}) async-start(f32[8,24,128]{2,1,0:T(8,128)} %summarize.1), calls=%async_computation | async-start | bytes 196608 | tf_op jit(solution)/shard_map/all_to_all | solution.py:380
  19.3 7.6 %all-to-all-done.pieces_ref = f32[8,24,128]{2,1,0:T(8,128)S(1)} async-done(((f32[8,24,128]{2,1,0:T(8,128)}), f32[8,24,128]{2,1,0:T(8,128)S(1)}, u32[]{:S(2)}, u32[]{:S(2)}) %all-to-all-start) | async-done | bytes 98336 | tf_op jit(solution)/shard_map/all_to_all | solution.py:380
  26.9 0.1 along.1
  26.9 17.3 %all_to_all.30.pieces_ref = f32[8,16,128]{2,1,0:T(8,128)S(1)} all-to-all(f32[8,16,128]{2,1,0:T(8,128)S(1)} %get-tuple-element.11), channel_id=1, replica_groups=mesh['sp_0'=8,'sp_1'=8,'x'=4,'core'=2] {'sp_0'}, dimensions={0} | all-to-all | bytes 131072 | tf_op jit(solution)/shard_map/all_to_all | solution.py:380
  44.3 0.1 across.1
  44.4 10.4 %all_to_all.31.pieces_ref = f32[8,24,128]{2,1,0:T(8,128)S(1)} all-to-all(f32[8,24,128]{2,1,0:T(8,128)S(1)} %across.1), channel_id=1, replica_groups=mesh['sp_0'=8,'sp_1'=8,'x'=4,'core'=2] {'sp_1'}, dimensions={0} | all-to-all | bytes 196608 | tf_op jit(solution)/shard_map/all_to_all | solution.py:380
  54.8 3.9 %mix.1 = bf16[256,2048]{1,0:T(8,128)(2,1)S(1)} custom-call(f32[8,24,128]{2,1,0:T(8,128)S(1)} %all_to_all.31.pieces_ref, bf16[256,128]{1,0:T(8,128)(2,1)} %query_ref.1, bf16[256,128]{1,0:T(8,128)(2,1)} %key_ref.3, bf16[256,128]{1,0:T(8,128)(2,1)} %value_ref.3, f32[2,2,256]{2,1,0:T(2,128)} %rate_ref.3, f32[2,2,256]{2,1,0:T(2,128)} %fusion.6.decay_ref, ...), custom_call_target="tpu_custom_call" | custom-call | tf_op jit(solution)/shard_map/mix/pallas_call | solution.py:364
  58.8 23.3 %all_to_all.32.pieces_ref = bf16[8,32,2048]{2,1,0:T(8,128)(2,1)S(1)} all-to-all(bf16[8,32,2048]{2,1,0:T(8,128)(2,1)S(1)} %bitcast.33), channel_id=1, replica_groups=mesh['sp_0'=8,'sp_1'=8,'x'=4,'core'=2] {'x','core'}, dimensions={0} | all-to-all | bytes 2097152 | tf_op jit(solution)/shard_map/all_to_all | solution.py:380
  82.1 1.7 %norm.1 = (bf16[32,2048]{1,0:T(8,128)(2,1)}, bf16[8,32,2048]{2,1,0:T(8,128)(2,1)S(1)}) custom-call(bf16[8,32,2048]{2,1,0:T(8,128)(2,1)S(1)} %all_to_all.32.pieces_ref, bf16[32,2048]{1,0:T(8,128)(2,1)} %skip_ref.1, f32[1,2048]{1,0:T(1,128)} %bitcast.35), custom_call_target="tpu_custom_call" | custom-call | tf_op jit(solution)/shard_map/norm/pallas_call | solution.py:364
  83.8 0.0 copy-start
  83.8 18.5 %all_to_all.33 = bf16[8,32,2048]{2,1,0:T(8,128)(2,1)S(1)} all-to-all(bf16[8,32,2048]{2,1,0:T(8,128)(2,1)S(1)} %get-tuple-element.14), channel_id=1, replica_groups=mesh['sp_0'=8,'sp_1'=8,'x'=4,'core'=2] {'x','core'}, dimensions={0} | all-to-all | bytes 2097152 | tf_op jit(solution)/shard_map/all_to_all | solution.py:380
  102.3 1.3 collective-permute-start
  103.6 4.0 %collective-permute-start.1 = (bf16[1,2048]{1,0:T(2,128)(2,1)S(1)}, bf16[1,2048]{1,0:T(2,128)(2,1)S(1)}, u32[]{:S(2)}, u32[]{:S(2)}) collective-permute-start(bf16[1,2048]{1,0:T(2,128)(2,1)S(1)} %get-tuple-element.18), channel_id=1, source_target_pairs={{0,8},{8,16},{16,24},{24,32},{32,40},{40,48},{48,56},{56,64},{64,7... | collective-permute-start | bytes 12296 | tf_op jit(solution)/shard_map/ppermute | solution.py:450
  107.6 0.1 pad.7.clone
  107.7 1.3 pad.4.taps_ref
  109.0 0.0 collective-permute-done
  109.0 0.0 collective-permute-done.1
  109.0 0.1 maximum_maximum_fusion.edges_ref
  109.1 9.1 %all-gather.2.cloned.1.call-done.weight_ref = bf16[2048,2176]{1,0:T(8,128)(2,1)} async-done(((bf16[32,2176]{1,0:T(8,128)(2,1)}), bf16[2048,2176]{1,0:T(8,128)(2,1)}) %all-gather.2.cloned.1.call-update) | async-done | bytes 8912912 | tf_op jit(solution)/shard_map/all_gather | solution.py:406
  118.2 6.1 %feed.1 = (bf16[4,32,2048]{2,1,0:T(8,128)(2,1)S(1)}, bf16[4,32,2048]{2,1,0:T(8,128)(2,1)S(1)}) custom-call(s32[1]{0:T(128)} %bitcast.4.core_ref, bf16[256,2048]{1,0:T(8,128)(2,1)S(1)} %bitcast.32, bf16[16,2048]{1,0:T(8,128)(2,1)S(1)} %maximum_maximum_fusion.edges_ref, bf16[2048,2176]{1,0:T(8,128)(2,1)} %all-gather.2.cloned.1.call-done.weight_ref, ...), custom_call_target="tpu_custom_call" | custom-call | tf_op jit(solution)/shard_map/feed/pallas_call | solution.py:455
  124.3 2.7 %collective-permute-start.2 = (bf16[4,32,2048]{2,1,0:T(8,128)(2,1)S(1)}, bf16[4,32,2048]{2,1,0:T(8,128)(2,1)S(1)}, u32[]{:S(2)}, u32[]{:S(2)}) collective-permute-start(bf16[4,32,2048]{2,1,0:T(8,128)(2,1)S(1)} %get-tuple-element.16), channel_id=1, source_target_pairs={{0,1},{1,0},{2,3},{3,2},{4,5},{5,4},{6,7},{7,6},{8,9},{9,8},{10,11... | collective-permute-start | bytes 1572872 | tf_op jit(solution)/shard_map/ppermute | solution.py:474
  127.0 1.5 %collective-permute-done.2 = bf16[4,32,2048]{2,1,0:T(8,128)(2,1)S(1)} collective-permute-done((bf16[4,32,2048]{2,1,0:T(8,128)(2,1)S(1)}, bf16[4,32,2048]{2,1,0:T(8,128)(2,1)S(1)}, u32[]{:S(2)}, u32[]{:S(2)}) %collective-permute-start.2) | collective-permute-done | bytes 524320 | tf_op jit(solution)/shard_map/ppermute | solution.py:474
  128.6 0.1 add_convert_fusion
  128.7 12.4 %all_to_all.34 = bf16[4,32,2048]{2,1,0:T(8,128)(2,1)S(1)} all-to-all(bf16[4,32,2048]{2,1,0:T(8,128)(2,1)S(1)} %add_convert_fusion), channel_id=1, replica_groups=mesh['sp_0'=8,'sp_1'=8,'x'=4,'core'=2] {'x'}, dimensions={0} | all-to-all | bytes 1048576 | tf_op jit(solution)/shard_map/all_to_all | solution.py:380
  141.1 0.1 convert_element_type.24
  141.2 0.0 copy-done
  141.2 0.7 fusion.1
  (2 shorter events, 0.0 us)
Async XLA Ops:
  6.5 111.7 %all-gather.2.cloned.1.call-start = ((), (), s32[]{:S(2)}) async-start(), calls=%async_computation.6 | async-start | bytes 9052160 | tf_op jit(solution)/shard_map/all_gather | solution.py:406
  11.7 15.2 %all-to-all-start = ((f32[8,24,128]{2,1,0:T(8,128)}), f32[8,24,128]{2,1,0:T(8,128)S(1)}, u32[]{:S(2)}, u32[]{:S(2)}) async-start(f32[8,24,128]{2,1,0:T(8,128)} %summarize.1), calls=%async_computation | async-start | bytes 196608 | tf_op jit(solution)/shard_map/all_to_all | solution.py:380
  83.8 57.4 %copy-start = (bf16[32,2048]{1,0:T(8,128)(2,1)S(1)}, bf16[32,2048]{1,0:T(8,128)(2,1)}, u32[]{:S(2)}) copy-start(bf16[32,2048]{1,0:T(8,128)(2,1)} %get-tuple-element.13) | copy-start | bytes 393220
  102.3 6.7 %collective-permute-start = (bf16[1,2048]{1,0:T(2,128)(2,1)S(1)}, bf16[1,2048]{1,0:T(2,128)(2,1)S(1)}, u32[]{:S(2)}, u32[]{:S(2)}) collective-permute-start(bf16[1,2048]{1,0:T(2,128)(2,1)S(1)} %get-tuple-element.17), channel_id=1, source_target_pairs={{8,0},{16,8},{24,16},{32,24},{40,32},{48,40},{56,48},{64,56},{72,6... | collective-permute-start | bytes 12296 | tf_op jit(solution)/shard_map/ppermute | solution.py:451
  103.6 5.4 %collective-permute-start.1 = (bf16[1,2048]{1,0:T(2,128)(2,1)S(1)}, bf16[1,2048]{1,0:T(2,128)(2,1)S(1)}, u32[]{:S(2)}, u32[]{:S(2)}) collective-permute-start(bf16[1,2048]{1,0:T(2,128)(2,1)S(1)} %get-tuple-element.18), channel_id=1, source_target_pairs={{0,8},{8,16},{16,24},{24,32},{32,40},{40,48},{48,56},{56,64},{64,7... | collective-permute-start | bytes 12296 | tf_op jit(solution)/shard_map/ppermute | solution.py:450
  124.3 4.3 %collective-permute-start.2 = (bf16[4,32,2048]{2,1,0:T(8,128)(2,1)S(1)}, bf16[4,32,2048]{2,1,0:T(8,128)(2,1)S(1)}, u32[]{:S(2)}, u32[]{:S(2)}) collective-permute-start(bf16[4,32,2048]{2,1,0:T(8,128)(2,1)S(1)} %get-tuple-element.16), channel_id=1, source_target_pairs={{0,1},{1,0},{2,3},{3,2},{4,5},{5,4},{6,7},{7,6},{8,9},{9,8},{10,11... | collective-permute-start | bytes 1572872 | tf_op jit(solution)/shard_map/ppermute | solution.py:474
Sparse Core Ops, SparseCore 0:
  10.3 107.8 all-gather.1

commit v3 on v2

--- a/solution.py
+++ b/solution.py
@@ -18,7 +18,8 @@
 GATE_AT = MAIN + 128
 DOWN_AT = GATE_AT + MAIN
 PACKED = DOWN_AT + 768
-FEED_STEPS = 4
+FEED_STEPS = 2
+FEED_COLS = 256
 ANY = pl.BlockSpec(memory_space=pl.ANY)
 f32 = jnp.float32
 bf16 = jnp.bfloat16
@@ -332,7 +333,7 @@
     rows_ref[:length, :] = tokens_ref[...]
     rows_ref[length:, :] = edges_ref[...]
     inner, gate = None, None
-    for i in range(FEED_STEPS):
+    for i in range(FEED_STEPS - 1):
         copies[i].wait()
         rows = slice(i * step, (i + 1) * step)
         left = rows_ref[:, rows]
@@ -340,13 +341,22 @@
         second = dot(left[:length], loaded_ref[rows, GATE_AT:DOWN_AT])
         inner = first if inner is None else inner + first
         gate = second if gate is None else gate + second
-    rounded = inner.astype(bf16).astype(f32)
-    hidden = gated(rounded[:, :MAIN], gate, taps_ref[:, :MAIN])
-    keep(hidden, slice(0, MAIN))
-    gate = pltpu.roll(inner[:length, MAIN:], 64, 1)
-    hidden = gated(rounded[:, MAIN:], gate, taps_ref[:, MAIN:])
-    hidden = jnp.where(iota(hidden.shape, 1) < HIDDEN - MAIN, hidden, 0.0)
-    keep(hidden, slice(MAIN, None))
+    copies[FEED_STEPS - 1].wait()
+    rows = slice(width - step, width)
+    left = rows_ref[:, rows]
+    for at in range(0, GATE_AT, FEED_COLS):
+        end = at + FEED_COLS
+        stop = min(end, MAIN)
+        up = inner[:, at:end] + dot(left, loaded_ref[rows, at:end])
+        weight = loaded_ref[rows, GATE_AT + at : GATE_AT + stop]
+        by = gate[:, at:stop] + dot(left[:length], weight)
+        rounded = up.astype(bf16).astype(f32)
+        keep(gated(rounded[:, : stop - at], by, taps_ref[:, at:stop]), slice(at, stop))
+        if end > MAIN:
+            by = pltpu.roll(up[:length, stop - at :], 64, 1)
+            hidden = gated(rounded[:, stop - at :], by, taps_ref[:, MAIN:])
+            hidden = jnp.where(iota(hidden.shape, 1) < HIDDEN - MAIN, hidden, 0.0)
+            keep(hidden, slice(MAIN, None))
     copies[FEED_STEPS].wait()
     for at in range(0, width, 256):
         cols = slice(at, at + 256)

time: 150 us -> 149 us (level)
  no operation moved by 1% of the time
where the time goes in v3:
time: 149 us; the launch traced here: 148 us
  blocking collectives  82 us (55%)
  waiting for transfers between devices  18.2 us (12%)
  starting transfers between devices  15.7 us (11%)
  Pallas kernels  15.4 us (10%)
  between operations  13.5 us (9%)
  other arithmetic  2.34 us (2%)
    all_to_all x5, blocking collectives, exchanged(): return lax.all_to_all(pieces, axis, split_axis=0, concat_axis=0, tiled=True)  82 us
    pallas_call x6, Pallas kernels, call(): pl.pallas_call(kernel, out_shape=out_shape, in_specs=in_specs, out_specs=...  9.63 us
    all_gather x1, waiting for transfers between devices, body(): weights = lax.all_gather(packed, SP, axis=0, tiled=True)  9.11 us
    all_to_all x1, starting transfers between devices, exchanged(): return lax.all_to_all(pieces, axis, split_axis=0, concat_axis=0, tiled=True)  7.64 us
    all_to_all x1, waiting for transfers between devices, exchanged(): return lax.all_to_all(pieces, axis, split_axis=0, concat_axis=0, tiled=True)  7.58 us
    pallas_call x1, Pallas kernels, body(): pl.pallas_call(feed_kernel, out_shape=(halves, halves), in_specs=[SMEM, V...  5.78 us
    ppermute x1, starting transfers between devices, body(): earlier = lax.ppermute(tokens[length - 1:], SP, up)  3.99 us
  transfers between devices with their start and end apart: 5, of which 3 were waited for; matrix products, arithmetic and copies ran while one was open for 2% of the time, Pallas kernels for 5%

profile of v3, /device:TPU:1, one launch (start us, length us, event | category | flops | bytes accessed | tf_op | source)
XLA Modules:
  0.0 148.5 jit_solution(5332474081736704761)
XLA Ops:
  6.5 0.0 all-gather.2.cloned.1.call-start
  6.5 1.6 %pack.1 = bf16[32,2176]{1,0:T(8,128)(2,1)} custom-call(bf16[32,704]{1,0:T(8,128)(2,1)} %up_ref.1, bf16[32,704]{1,0:T(8,128)(2,1)} %gate_ref.1, bf16[32,704]{1,0:T(8,128)(2,1)} %bitcast.34), custom_call_target="tpu_custom_call" | custom-call | tf_op jit(solution)/shard_map/pack/pallas_call | solution.py:374
  8.1 0.0 all-gather.2.cloned.1.call-update
  8.1 1.3 fusion.6.decay_ref
  9.5 2.2 %summarize.1 = f32[8,24,128]{2,1,0:T(8,128)} custom-call(bf16[256,128]{1,0:T(8,128)(2,1)} %key_ref.3, bf16[256,128]{1,0:T(8,128)(2,1)} %value_ref.3, f32[2,2,256]{2,1,0:T(2,128)} %rate_ref.3, f32[2,2,256]{2,1,0:T(2,128)} %fusion.6.decay_ref), custom_call_target="tpu_custom_call" | custom-call | tf_op jit(solution)/shard_map/summarize/pallas_call | solution.py:374
  11.7 7.6 %all-to-all-start = ((f32[8,24,128]{2,1,0:T(8,128)}), f32[8,24,128]{2,1,0:T(8,128)S(1)}, u32[]{:S(2)}, u32[]{:S(2)}) async-start(f32[8,24,128]{2,1,0:T(8,128)} %summarize.1), calls=%async_computation | async-start | bytes 196608 | tf_op jit(solution)/shard_map/all_to_all | solution.py:390
  19.3 7.6 %all-to-all-done.pieces_ref = f32[8,24,128]{2,1,0:T(8,128)S(1)} async-done(((f32[8,24,128]{2,1,0:T(8,128)}), f32[8,24,128]{2,1,0:T(8,128)S(1)}, u32[]{:S(2)}, u32[]{:S(2)}) %all-to-all-start) | async-done | bytes 98336 | tf_op jit(solution)/shard_map/all_to_all | solution.py:390
  26.9 0.1 along.1
  26.9 17.3 %all_to_all.30.pieces_ref = f32[8,16,128]{2,1,0:T(8,128)S(1)} all-to-all(f32[8,16,128]{2,1,0:T(8,128)S(1)} %get-tuple-element.11), channel_id=1, replica_groups=mesh['sp_0'=8,'sp_1'=8,'x'=4,'core'=2] {'sp_0'}, dimensions={0} | all-to-all | bytes 131072 | tf_op jit(solution)/shard_map/all_to_all | solution.py:390
  44.3 0.1 across.1
  44.4 10.4 %all_to_all.31.pieces_ref = f32[8,24,128]{2,1,0:T(8,128)S(1)} all-to-all(f32[8,24,128]{2,1,0:T(8,128)S(1)} %across.1), channel_id=1, replica_groups=mesh['sp_0'=8,'sp_1'=8,'x'=4,'core'=2] {'sp_1'}, dimensions={0} | all-to-all | bytes 196608 | tf_op jit(solution)/shard_map/all_to_all | solution.py:390
  54.8 3.9 %mix.1 = bf16[256,2048]{1,0:T(8,128)(2,1)S(1)} custom-call(f32[8,24,128]{2,1,0:T(8,128)S(1)} %all_to_all.31.pieces_ref, bf16[256,128]{1,0:T(8,128)(2,1)} %query_ref.1, bf16[256,128]{1,0:T(8,128)(2,1)} %key_ref.3, bf16[256,128]{1,0:T(8,128)(2,1)} %value_ref.3, f32[2,2,256]{2,1,0:T(2,128)} %rate_ref.3, f32[2,2,256]{2,1,0:T(2,128)} %fusion.6.decay_ref, ...), custom_call_target="tpu_custom_call" | custom-call | tf_op jit(solution)/shard_map/mix/pallas_call | solution.py:374
  58.8 23.3 %all_to_all.32.pieces_ref = bf16[8,32,2048]{2,1,0:T(8,128)(2,1)S(1)} all-to-all(bf16[8,32,2048]{2,1,0:T(8,128)(2,1)S(1)} %bitcast.33), channel_id=1, replica_groups=mesh['sp_0'=8,'sp_1'=8,'x'=4,'core'=2] {'x','core'}, dimensions={0} | all-to-all | bytes 2097152 | tf_op jit(solution)/shard_map/all_to_all | solution.py:390
  82.1 1.7 %norm.1 = (bf16[32,2048]{1,0:T(8,128)(2,1)}, bf16[8,32,2048]{2,1,0:T(8,128)(2,1)S(1)}) custom-call(bf16[8,32,2048]{2,1,0:T(8,128)(2,1)S(1)} %all_to_all.32.pieces_ref, bf16[32,2048]{1,0:T(8,128)(2,1)} %skip_ref.1, f32[1,2048]{1,0:T(1,128)} %bitcast.35), custom_call_target="tpu_custom_call" | custom-call | tf_op jit(solution)/shard_map/norm/pallas_call | solution.py:374
  83.8 0.0 copy-start
  83.8 18.5 %all_to_all.33 = bf16[8,32,2048]{2,1,0:T(8,128)(2,1)S(1)} all-to-all(bf16[8,32,2048]{2,1,0:T(8,128)(2,1)S(1)} %get-tuple-element.14), channel_id=1, replica_groups=mesh['sp_0'=8,'sp_1'=8,'x'=4,'core'=2] {'x','core'}, dimensions={0} | all-to-all | bytes 2097152 | tf_op jit(solution)/shard_map/all_to_all | solution.py:390
  102.3 1.3 collective-permute-start
  103.6 4.0 %collective-permute-start.1 = (bf16[1,2048]{1,0:T(2,128)(2,1)S(1)}, bf16[1,2048]{1,0:T(2,128)(2,1)S(1)}, u32[]{:S(2)}, u32[]{:S(2)}) collective-permute-start(bf16[1,2048]{1,0:T(2,128)(2,1)S(1)} %get-tuple-element.18), channel_id=1, source_target_pairs={{0,8},{8,16},{16,24},{24,32},{32,40},{40,48},{48,56},{56,64},{64,7... | collective-permute-start | bytes 12296 | tf_op jit(solution)/shard_map/ppermute | solution.py:460
  107.6 0.1 pad.7.clone
  107.7 1.3 pad.4.taps_ref
  109.0 0.0 collective-permute-done
  109.0 0.0 collective-permute-done.1
  109.0 0.1 maximum_maximum_fusion.edges_ref
  109.1 9.1 %all-gather.2.cloned.1.call-done.weight_ref = bf16[2048,2176]{1,0:T(8,128)(2,1)} async-done(((bf16[32,2176]{1,0:T(8,128)(2,1)}), bf16[2048,2176]{1,0:T(8,128)(2,1)}) %all-gather.2.cloned.1.call-update) | async-done | bytes 8912912 | tf_op jit(solution)/shard_map/all_gather | solution.py:416
  118.2 5.8 %feed.1 = (bf16[4,32,2048]{2,1,0:T(8,128)(2,1)S(1)}, bf16[4,32,2048]{2,1,0:T(8,128)(2,1)S(1)}) custom-call(s32[1]{0:T(128)} %bitcast.4.core_ref, bf16[256,2048]{1,0:T(8,128)(2,1)S(1)} %bitcast.32, bf16[16,2048]{1,0:T(8,128)(2,1)S(1)} %maximum_maximum_fusion.edges_ref, bf16[2048,2176]{1,0:T(8,128)(2,1)} %all-gather.2.cloned.1.call-done.weight_ref, ...), custom_call_target="tpu_custom_call" | custom-call | tf_op jit(solution)/shard_map/feed/pallas_call | solution.py:465
  124.0 2.8 %collective-permute-start.2 = (bf16[4,32,2048]{2,1,0:T(8,128)(2,1)S(1)}, bf16[4,32,2048]{2,1,0:T(8,128)(2,1)S(1)}, u32[]{:S(2)}, u32[]{:S(2)}) collective-permute-start(bf16[4,32,2048]{2,1,0:T(8,128)(2,1)S(1)} %get-tuple-element.16), channel_id=1, source_target_pairs={{0,1},{1,0},{2,3},{3,2},{4,5},{5,4},{6,7},{7,6},{8,9},{9,8},{10,11... | collective-permute-start | bytes 1572872 | tf_op jit(solution)/shard_map/ppermute | solution.py:484
  126.8 1.5 %collective-permute-done.2 = bf16[4,32,2048]{2,1,0:T(8,128)(2,1)S(1)} collective-permute-done((bf16[4,32,2048]{2,1,0:T(8,128)(2,1)S(1)}, bf16[4,32,2048]{2,1,0:T(8,128)(2,1)S(1)}, u32[]{:S(2)}, u32[]{:S(2)}) %collective-permute-start.2) | collective-permute-done | bytes 524320 | tf_op jit(solution)/shard_map/ppermute | solution.py:484
  128.3 0.1 add_convert_fusion
  128.4 12.4 %all_to_all.34 = bf16[4,32,2048]{2,1,0:T(8,128)(2,1)S(1)} all-to-all(bf16[4,32,2048]{2,1,0:T(8,128)(2,1)S(1)} %add_convert_fusion), channel_id=1, replica_groups=mesh['sp_0'=8,'sp_1'=8,'x'=4,'core'=2] {'x'}, dimensions={0} | all-to-all | bytes 1048576 | tf_op jit(solution)/shard_map/all_to_all | solution.py:390
  140.8 0.1 convert_element_type.24
  140.9 0.0 copy-done
  140.9 0.7 fusion.1
  (2 shorter events, 0.0 us)
Async XLA Ops:
  6.5 111.7 %all-gather.2.cloned.1.call-start = ((), (), s32[]{:S(2)}) async-start(), calls=%async_computation.6 | async-start | bytes 9052160 | tf_op jit(solution)/shard_map/all_gather | solution.py:416
  11.7 15.2 %all-to-all-start = ((f32[8,24,128]{2,1,0:T(8,128)}), f32[8,24,128]{2,1,0:T(8,128)S(1)}, u32[]{:S(2)}, u32[]{:S(2)}) async-start(f32[8,24,128]{2,1,0:T(8,128)} %summarize.1), calls=%async_computation | async-start | bytes 196608 | tf_op jit(solution)/shard_map/all_to_all | solution.py:390
  83.8 57.1 %copy-start = (bf16[32,2048]{1,0:T(8,128)(2,1)S(1)}, bf16[32,2048]{1,0:T(8,128)(2,1)}, u32[]{:S(2)}) copy-start(bf16[32,2048]{1,0:T(8,128)(2,1)} %get-tuple-element.13) | copy-start | bytes 393220
  102.3 6.7 %collective-permute-start = (bf16[1,2048]{1,0:T(2,128)(2,1)S(1)}, bf16[1,2048]{1,0:T(2,128)(2,1)S(1)}, u32[]{:S(2)}, u32[]{:S(2)}) collective-permute-start(bf16[1,2048]{1,0:T(2,128)(2,1)S(1)} %get-tuple-element.17), channel_id=1, source_target_pairs={{8,0},{16,8},{24,16},{32,24},{40,32},{48,40},{56,48},{64,56},{72,6... | collective-permute-start | bytes 12296 | tf_op jit(solution)/shard_map/ppermute | solution.py:461
  103.6 5.4 %collective-permute-start.1 = (bf16[1,2048]{1,0:T(2,128)(2,1)S(1)}, bf16[1,2048]{1,0:T(2,128)(2,1)S(1)}, u32[]{:S(2)}, u32[]{:S(2)}) collective-permute-start(bf16[1,2048]{1,0:T(2,128)(2,1)S(1)} %get-tuple-element.18), channel_id=1, source_target_pairs={{0,8},{8,16},{16,24},{24,32},{32,40},{40,48},{48,56},{56,64},{64,7... | collective-permute-start | bytes 12296 | tf_op jit(solution)/shard_map/ppermute | solution.py:460
  124.0 4.3 %collective-permute-start.2 = (bf16[4,32,2048]{2,1,0:T(8,128)(2,1)S(1)}, bf16[4,32,2048]{2,1,0:T(8,128)(2,1)S(1)}, u32[]{:S(2)}, u32[]{:S(2)}) collective-permute-start(bf16[4,32,2048]{2,1,0:T(8,128)(2,1)S(1)} %get-tuple-element.16), channel_id=1, source_target_pairs={{0,1},{1,0},{2,3},{3,2},{4,5},{5,4},{6,7},{7,6},{8,9},{9,8},{10,11... | collective-permute-start | bytes 1572872 | tf_op jit(solution)/shard_map/ppermute | solution.py:484
Sparse Core Ops, SparseCore 0:
  10.3 107.8 all-gather.1

commit v4 on v3

--- a/solution.py
+++ b/solution.py
@@ -302,15 +302,15 @@
     edges_ref,
     weight_ref,
     taps_ref,
-    own_ref,
     other_ref,
+    hidden_ref,
+    down_ref,
     rows_ref,
     loaded_ref,
-    hidden_ref,
     sems,
 ):
     length, width = tokens_ref.shape
-    pairs, own, _ = own_ref.shape
+    pairs, own, _ = other_ref.shape
 
     def keep(hidden, cols):
         for x in range(pairs):
@@ -323,12 +323,11 @@
     step = width // FEED_STEPS
     copies = []
     for i in range(FEED_STEPS + 1):
-        place = (pl.ds(i * step, step), pl.ds(0, DOWN_AT))
+        place, target = (pl.ds(i * step, step), pl.ds(0, DOWN_AT)), loaded_ref
         if i == FEED_STEPS:
-            place = (pl.ds(0, width), pl.ds(DOWN_AT, PACKED - DOWN_AT))
-        copies.append(
-            pltpu.make_async_copy(weight_ref.at[place], loaded_ref.at[place], sems.at[i])
-        )
+            place, target = (pl.ds(0, width), pl.ds(DOWN_AT, PACKED - DOWN_AT)), down_ref
+        target = target if i == FEED_STEPS else target.at[place]
+        copies.append(pltpu.make_async_copy(weight_ref.at[place], target, sems.at[i]))
         copies[i].start()
     rows_ref[:length, :] = tokens_ref[...]
     rows_ref[length:, :] = edges_ref[...]
@@ -358,11 +357,18 @@
             hidden = jnp.where(iota(hidden.shape, 1) < HIDDEN - MAIN, hidden, 0.0)
             keep(hidden, slice(MAIN, None))
     copies[FEED_STEPS].wait()
-    for at in range(0, width, 256):
+    lowered(other_ref, hidden_ref[length // 2 :, :], down_ref)
+
+
+def lowered(out_ref, hidden, down_ref):
+    for at in range(0, down_ref.shape[0], 256):
         cols = slice(at, at + 256)
-        part = dot(hidden_ref[...], loaded_ref[cols, DOWN_AT:], ((1,), (1,))).astype(bf16)
-        own_ref[:, :, cols] = part[: length // 2].reshape(pairs, own, 256)
-        other_ref[:, :, cols] = part[length // 2 :].reshape(pairs, own, 256)
+        part = dot(hidden, down_ref[cols, :], ((1,), (1,))).astype(bf16)
+        out_ref[:, :, cols] = part.reshape(out_ref.shape[0], out_ref.shape[1], 256)
+
+
+def own_kernel(hidden_ref, down_ref, out_ref):
+    lowered(out_ref, hidden_ref[: hidden_ref.shape[0] // 2, :], down_ref)
 
 
 def near(x):
@@ -462,17 +468,21 @@
     edges = jnp.concatenate([later, earlier, jnp.zeros((14, width), bf16)], axis=0)
 
     halves = pltpu.VMEM((members // 2, own, width), bf16)
-    own_half, other_half = pl.pallas_call(
+    other_half, hidden, down_part = pl.pallas_call(
         feed_kernel,
-        out_shape=(halves, halves),
+        out_shape=(
+            halves,
+            pltpu.VMEM((length, 768), bf16),
+            pltpu.VMEM((width, PACKED - DOWN_AT), bf16),
+        ),
         in_specs=[SMEM, VMEM, VMEM, ANY, VMEM],
-        out_specs=(VMEM, VMEM),
+        out_specs=(VMEM, VMEM, VMEM),
         scratch_shapes=[
             pltpu.VMEM((length + 16, width), bf16),
-            pltpu.VMEM((width, PACKED), bf16),
-            pltpu.VMEM((length, 768), bf16),
+            pltpu.VMEM((width, DOWN_AT), bf16),
             pltpu.SemaphoreType.DMA((FEED_STEPS + 1,)),
         ],
+        compiler_params=pltpu.CompilerParams(vmem_limit_bytes=40 * 2**20),
         name="feed",
     )(
         lax.axis_index("core").reshape(1),
@@ -482,6 +492,14 @@
         jnp.pad(neighbour_filter_coefficients, ((0, 0), (0, 768 - HIDDEN))),
     )
     from_partner = lax.ppermute(other_half, "core", [(0, 1), (1, 0)])
+    own_half = pl.pallas_call(
+        own_kernel,
+        out_shape=halves,
+        in_specs=[VMEM] * 2,
+        out_specs=VMEM,
+        compiler_params=pltpu.CompilerParams(vmem_limit_bytes=40 * 2**20),
+        name="own",
+    )(near(hidden), near(down_part))
     pair = (own_half.astype(f32) + from_partner.astype(f32)).astype(bf16)
     pieces = exchanged(pair, "x").astype(f32)
     total = middle.astype(f32)

time: 149 us -> 149 us (level)
    pallas_call x1 -> x2, Pallas kernels: 5.78 us -> 6.37 us  [the longest x1 5.23 us: body(): pl.pallas_call(feed_kernel, out_shape=(halves, pltpu.VMEM((length, 768),...]
  transfers between devices with their start and end apart: 5 -> 5, of which waited for: 3 -> 3; matrix products, arithmetic and copies ran while one was open for 2% -> 1% of each run, Pallas kernels for 5% -> 6%
where the time goes in v4:
time: 149 us; the launch traced here: 148 us
  blocking collectives  81.8 us (55%)
  waiting for transfers between devices  17.8 us (12%)
  Pallas kernels  16 us (11%)
  starting transfers between devices  15.7 us (11%)
  between operations  13.5 us (9%)
  other arithmetic  2.35 us (2%)
    all_to_all x5, blocking collectives, exchanged(): return lax.all_to_all(pieces, axis, split_axis=0, concat_axis=0, tiled=True)  81.8 us
    all_gather x1, waiting for transfers between devices, body(): weights = lax.all_gather(packed, SP, axis=0, tiled=True)  9.84 us
    pallas_call x6, Pallas kernels, call(): pl.pallas_call(kernel, out_shape=out_shape, in_specs=in_specs, out_specs=...  9.63 us
    all_to_all x1, starting transfers between devices, exchanged(): return lax.all_to_all(pieces, axis, split_axis=0, concat_axis=0, tiled=True)  7.64 us
    all_to_all x1, waiting for transfers between devices, exchanged(): return lax.all_to_all(pieces, axis, split_axis=0, concat_axis=0, tiled=True)  7.58 us
    pallas_call x1, Pallas kernels, body(): pl.pallas_call(feed_kernel, out_shape=(halves, pltpu.VMEM((length, 768),...  5.23 us
    ppermute x1, starting transfers between devices, body(): earlier = lax.ppermute(tokens[length - 1:], SP, up)  3.99 us
  transfers between devices with their start and end apart: 5, of which 3 were waited for; matrix products, arithmetic and copies ran while one was open for 1% of the time, Pallas kernels for 6%

profile of v4, /device:TPU:1, one launch (start us, length us, event | category | flops | bytes accessed | tf_op | source)
XLA Modules:
  0.0 147.9 jit_solution(4798168445350028639)
XLA Ops:
  6.5 0.0 all-gather.2.cloned.1.call-start
  6.5 1.6 %pack.1 = bf16[32,2176]{1,0:T(8,128)(2,1)} custom-call(bf16[32,704]{1,0:T(8,128)(2,1)} %up_ref.1, bf16[32,704]{1,0:T(8,128)(2,1)} %gate_ref.1, bf16[32,704]{1,0:T(8,128)(2,1)} %bitcast.34), custom_call_target="tpu_custom_call" | custom-call | tf_op jit(solution)/shard_map/pack/pallas_call | solution.py:380
  8.1 0.0 all-gather.2.cloned.1.call-update
  8.1 1.3 fusion.6.decay_ref
  9.5 2.2 %summarize.1 = f32[8,24,128]{2,1,0:T(8,128)} custom-call(bf16[256,128]{1,0:T(8,128)(2,1)} %key_ref.3, bf16[256,128]{1,0:T(8,128)(2,1)} %value_ref.3, f32[2,2,256]{2,1,0:T(2,128)} %rate_ref.3, f32[2,2,256]{2,1,0:T(2,128)} %fusion.6.decay_ref), custom_call_target="tpu_custom_call" | custom-call | tf_op jit(solution)/shard_map/summarize/pallas_call | solution.py:380
  11.7 7.6 %all-to-all-start = ((f32[8,24,128]{2,1,0:T(8,128)}), f32[8,24,128]{2,1,0:T(8,128)S(1)}, u32[]{:S(2)}, u32[]{:S(2)}) async-start(f32[8,24,128]{2,1,0:T(8,128)} %summarize.1), calls=%async_computation | async-start | bytes 196608 | tf_op jit(solution)/shard_map/all_to_all | solution.py:396
  19.3 7.6 %all-to-all-done.pieces_ref = f32[8,24,128]{2,1,0:T(8,128)S(1)} async-done(((f32[8,24,128]{2,1,0:T(8,128)}), f32[8,24,128]{2,1,0:T(8,128)S(1)}, u32[]{:S(2)}, u32[]{:S(2)}) %all-to-all-start) | async-done | bytes 98336 | tf_op jit(solution)/shard_map/all_to_all | solution.py:396
  26.9 0.1 along.1
  26.9 17.3 %all_to_all.30.pieces_ref = f32[8,16,128]{2,1,0:T(8,128)S(1)} all-to-all(f32[8,16,128]{2,1,0:T(8,128)S(1)} %get-tuple-element.12), channel_id=1, replica_groups=mesh['sp_0'=8,'sp_1'=8,'x'=4,'core'=2] {'sp_0'}, dimensions={0} | all-to-all | bytes 131072 | tf_op jit(solution)/shard_map/all_to_all | solution.py:396
  44.3 0.1 across.1
  44.4 10.4 %all_to_all.31.pieces_ref = f32[8,24,128]{2,1,0:T(8,128)S(1)} all-to-all(f32[8,24,128]{2,1,0:T(8,128)S(1)} %across.1), channel_id=1, replica_groups=mesh['sp_0'=8,'sp_1'=8,'x'=4,'core'=2] {'sp_1'}, dimensions={0} | all-to-all | bytes 196608 | tf_op jit(solution)/shard_map/all_to_all | solution.py:396
  54.8 3.9 %mix.1 = bf16[256,2048]{1,0:T(8,128)(2,1)S(1)} custom-call(f32[8,24,128]{2,1,0:T(8,128)S(1)} %all_to_all.31.pieces_ref, bf16[256,128]{1,0:T(8,128)(2,1)} %query_ref.1, bf16[256,128]{1,0:T(8,128)(2,1)} %key_ref.3, bf16[256,128]{1,0:T(8,128)(2,1)} %value_ref.3, f32[2,2,256]{2,1,0:T(2,128)} %rate_ref.3, f32[2,2,256]{2,1,0:T(2,128)} %fusion.6.decay_ref, ...), custom_call_target="tpu_custom_call" | custom-call | tf_op jit(solution)/shard_map/mix/pallas_call | solution.py:380
  58.8 23.3 %all_to_all.32.pieces_ref = bf16[8,32,2048]{2,1,0:T(8,128)(2,1)S(1)} all-to-all(bf16[8,32,2048]{2,1,0:T(8,128)(2,1)S(1)} %bitcast.33), channel_id=1, replica_groups=mesh['sp_0'=8,'sp_1'=8,'x'=4,'core'=2] {'x','core'}, dimensions={0} | all-to-all | bytes 2097152 | tf_op jit(solution)/shard_map/all_to_all | solution.py:396
  82.1 1.7 %norm.1 = (bf16[32,2048]{1,0:T(8,128)(2,1)}, bf16[8,32,2048]{2,1,0:T(8,128)(2,1)S(1)}) custom-call(bf16[8,32,2048]{2,1,0:T(8,128)(2,1)S(1)} %all_to_all.32.pieces_ref, bf16[32,2048]{1,0:T(8,128)(2,1)} %skip_ref.1, f32[1,2048]{1,0:T(1,128)} %bitcast.35), custom_call_target="tpu_custom_call" | custom-call | tf_op jit(solution)/shard_map/norm/pallas_call | solution.py:380
  83.8 18.4 %all_to_all.33 = bf16[8,32,2048]{2,1,0:T(8,128)(2,1)S(1)} all-to-all(bf16[8,32,2048]{2,1,0:T(8,128)(2,1)S(1)} %get-tuple-element.15), channel_id=1, replica_groups=mesh['sp_0'=8,'sp_1'=8,'x'=4,'core'=2] {'x','core'}, dimensions={0} | all-to-all | bytes 2097152 | tf_op jit(solution)/shard_map/all_to_all | solution.py:396
  102.2 1.3 collective-permute-start
  103.5 4.0 %collective-permute-start.1 = (bf16[1,2048]{1,0:T(2,128)(2,1)S(1)}, bf16[1,2048]{1,0:T(2,128)(2,1)S(1)}, u32[]{:S(2)}, u32[]{:S(2)}) collective-permute-start(bf16[1,2048]{1,0:T(2,128)(2,1)S(1)} %get-tuple-element.20), channel_id=1, source_target_pairs={{0,8},{8,16},{16,24},{24,32},{32,40},{40,48},{48,56},{56,64},{64,7... | collective-permute-start | bytes 12296 | tf_op jit(solution)/shard_map/ppermute | solution.py:466
  107.5 0.1 pad.7.clone
  107.6 0.7 pad.4.taps_ref
  108.3 0.0 collective-permute-done
  108.3 0.0 collective-permute-done.1
  108.3 0.1 maximum_maximum_fusion.edges_ref
  108.4 9.8 %all-gather.2.cloned.1.call-done.weight_ref = bf16[2048,2176]{1,0:T(8,128)(2,1)} async-done(((bf16[32,2176]{1,0:T(8,128)(2,1)}), bf16[2048,2176]{1,0:T(8,128)(2,1)}) %all-gather.2.cloned.1.call-update) | async-done | bytes 8912912 | tf_op jit(solution)/shard_map/all_gather | solution.py:422
  118.2 0.0 copy-start
  118.2 5.2 %feed.1 = (bf16[4,32,2048]{2,1,0:T(8,128)(2,1)S(1)}, bf16[256,768]{1,0:T(8,128)(2,1)S(1)}, bf16[2048,768]{1,0:T(8,128)(2,1)S(1)}) custom-call(s32[1]{0:T(128)} %bitcast.4.core_ref, bf16[256,2048]{1,0:T(8,128)(2,1)S(1)} %bitcast.32, bf16[16,2048]{1,0:T(8,128)(2,1)S(1)} %maximum_maximum_fusion.edges_ref, ...), custom_call_target="tpu_custom_call" | custom-call | tf_op jit(solution)/shard_map/feed/pallas_call | solution.py:471
  123.5 2.7 %collective-permute-start.2 = (bf16[4,32,2048]{2,1,0:T(8,128)(2,1)S(1)}, bf16[4,32,2048]{2,1,0:T(8,128)(2,1)S(1)}, u32[]{:S(2)}, u32[]{:S(2)}) collective-permute-start(bf16[4,32,2048]{2,1,0:T(8,128)(2,1)S(1)} %get-tuple-element.18), channel_id=1, source_target_pairs={{0,1},{1,0},{2,3},{3,2},{4,5},{5,4},{6,7},{7,6},{8,9},{9,8},{10,11... | collective-permute-start | bytes 1572872 | tf_op jit(solution)/shard_map/ppermute | solution.py:494
  126.2 1.1 own.1
  127.4 0.4 collective-permute-done.2
  127.7 0.1 add_convert_fusion
  127.9 12.4 %all_to_all.34 = bf16[4,32,2048]{2,1,0:T(8,128)(2,1)S(1)} all-to-all(bf16[4,32,2048]{2,1,0:T(8,128)(2,1)S(1)} %add_convert_fusion), channel_id=1, replica_groups=mesh['sp_0'=8,'sp_1'=8,'x'=4,'core'=2] {'x'}, dimensions={0} | all-to-all | bytes 1048576 | tf_op jit(solution)/shard_map/all_to_all | solution.py:396
  140.2 0.1 convert_element_type.24
  140.3 0.0 copy-done
  140.4 0.7 fusion.1
  (2 shorter events, 0.0 us)
Async XLA Ops:
  6.5 111.7 %all-gather.2.cloned.1.call-start = ((), (), s32[]{:S(2)}) async-start(), calls=%async_computation.6 | async-start | bytes 9052160 | tf_op jit(solution)/shard_map/all_gather | solution.py:422
  11.7 15.2 %all-to-all-start = ((f32[8,24,128]{2,1,0:T(8,128)}), f32[8,24,128]{2,1,0:T(8,128)S(1)}, u32[]{:S(2)}, u32[]{:S(2)}) async-start(f32[8,24,128]{2,1,0:T(8,128)} %summarize.1), calls=%async_computation | async-start | bytes 196608 | tf_op jit(solution)/shard_map/all_to_all | solution.py:396
  102.2 6.1 %collective-permute-start = (bf16[1,2048]{1,0:T(2,128)(2,1)S(1)}, bf16[1,2048]{1,0:T(2,128)(2,1)S(1)}, u32[]{:S(2)}, u32[]{:S(2)}) collective-permute-start(bf16[1,2048]{1,0:T(2,128)(2,1)S(1)} %get-tuple-element.19), channel_id=1, source_target_pairs={{8,0},{16,8},{24,16},{32,24},{40,32},{48,40},{56,48},{64,56},{72,6... | collective-permute-start | bytes 12296 | tf_op jit(solution)/shard_map/ppermute | solution.py:467
  103.5 4.8 %collective-permute-start.1 = (bf16[1,2048]{1,0:T(2,128)(2,1)S(1)}, bf16[1,2048]{1,0:T(2,128)(2,1)S(1)}, u32[]{:S(2)}, u32[]{:S(2)}) collective-permute-start(bf16[1,2048]{1,0:T(2,128)(2,1)S(1)} %get-tuple-element.20), channel_id=1, source_target_pairs={{0,8},{8,16},{16,24},{24,32},{32,40},{40,48},{48,56},{56,64},{64,7... | collective-permute-start | bytes 12296 | tf_op jit(solution)/shard_map/ppermute | solution.py:466
  118.2 22.1 %copy-start = (bf16[32,2048]{1,0:T(8,128)(2,1)S(1)}, bf16[32,2048]{1,0:T(8,128)(2,1)}, u32[]{:S(2)}) copy-start(bf16[32,2048]{1,0:T(8,128)(2,1)} %get-tuple-element.14) | copy-start | bytes 393220
  123.5 4.3 %collective-permute-start.2 = (bf16[4,32,2048]{2,1,0:T(8,128)(2,1)S(1)}, bf16[4,32,2048]{2,1,0:T(8,128)(2,1)S(1)}, u32[]{:S(2)}, u32[]{:S(2)}) collective-permute-start(bf16[4,32,2048]{2,1,0:T(8,128)(2,1)S(1)} %get-tuple-element.18), channel_id=1, source_target_pairs={{0,1},{1,0},{2,3},{3,2},{4,5},{5,4},{6,7},{7,6},{8,9},{9,8},{10,11... | collective-permute-start | bytes 1572872 | tf_op jit(solution)/shard_map/ppermute | solution.py:494
Sparse Core Ops, SparseCore 0:
  10.3 107.8 all-gather.1

commit v5 on v4

--- a/solution.py
+++ b/solution.py
@@ -501,10 +501,10 @@
         name="own",
     )(near(hidden), near(down_part))
     pair = (own_half.astype(f32) + from_partner.astype(f32)).astype(bf16)
-    pieces = exchanged(pair, "x").astype(f32)
+    pieces = exchanged(pair, "x")
     total = middle.astype(f32)
     for j in range(pieces.shape[0]):
-        total = total + pieces[j]
+        total = total + pieces[j].astype(f32)
     return total.astype(bf16)
 
 

time: 149 us -> 149 us (level)
  no operation moved by 1% of the time
where the time goes in v5:
time: 149 us; the launch traced here: 148 us
  blocking collectives  81.8 us (55%)
  waiting for transfers between devices  17.7 us (12%)
  Pallas kernels  16 us (11%)
  starting transfers between devices  15.8 us (11%)
  between operations  13.5 us (9%)
  other arithmetic  2.27 us (2%)
    all_to_all x5, blocking collectives, exchanged(): return lax.all_to_all(pieces, axis, split_axis=0, concat_axis=0, tiled=True)  81.8 us
    all_gather x1, waiting for transfers between devices, body(): weights = lax.all_gather(packed, SP, axis=0, tiled=True)  9.7 us
    pallas_call x6, Pallas kernels, call(): pl.pallas_call(kernel, out_shape=out_shape, in_specs=in_specs, out_specs=...  9.63 us
    all_to_all x1, starting transfers between devices, exchanged(): return lax.all_to_all(pieces, axis, split_axis=0, concat_axis=0, tiled=True)  7.64 us
    all_to_all x1, waiting for transfers between devices, exchanged(): return lax.all_to_all(pieces, axis, split_axis=0, concat_axis=0, tiled=True)  7.58 us
    pallas_call x1, Pallas kernels, body(): pl.pallas_call(feed_kernel, out_shape=(halves, pltpu.VMEM((length, 768),...  5.19 us
    ppermute x1, starting transfers between devices, body(): earlier = lax.ppermute(tokens[length - 1:], SP, up)  3.99 us
  transfers between devices with their start and end apart: 5, of which 3 were waited for; matrix products, arithmetic and copies ran while one was open for 1% of the time, Pallas kernels for 6%

profile of v5, /device:TPU:1, one launch (start us, length us, event | category | flops | bytes accessed | tf_op | source)
XLA Modules:
  0.0 147.8 jit_solution(8013135186169551925)
XLA Ops:
  6.5 0.0 all-gather.2.cloned.1.call-start
  6.5 1.6 %pack.1 = bf16[32,2176]{1,0:T(8,128)(2,1)} custom-call(bf16[32,704]{1,0:T(8,128)(2,1)} %up_ref.1, bf16[32,704]{1,0:T(8,128)(2,1)} %gate_ref.1, bf16[32,704]{1,0:T(8,128)(2,1)} %bitcast.30), custom_call_target="tpu_custom_call" | custom-call | tf_op jit(solution)/shard_map/pack/pallas_call | solution.py:380
  8.1 0.0 all-gather.2.cloned.1.call-update
  8.1 1.3 fusion.2.decay_ref
  9.5 2.2 %summarize.1 = f32[8,24,128]{2,1,0:T(8,128)} custom-call(bf16[256,128]{1,0:T(8,128)(2,1)} %key_ref.3, bf16[256,128]{1,0:T(8,128)(2,1)} %value_ref.3, f32[2,2,256]{2,1,0:T(2,128)} %rate_ref.3, f32[2,2,256]{2,1,0:T(2,128)} %fusion.2.decay_ref), custom_call_target="tpu_custom_call" | custom-call | tf_op jit(solution)/shard_map/summarize/pallas_call | solution.py:380
  11.7 7.6 %all-to-all-start = ((f32[8,24,128]{2,1,0:T(8,128)}), f32[8,24,128]{2,1,0:T(8,128)S(1)}, u32[]{:S(2)}, u32[]{:S(2)}) async-start(f32[8,24,128]{2,1,0:T(8,128)} %summarize.1), calls=%async_computation | async-start | bytes 196608 | tf_op jit(solution)/shard_map/all_to_all | solution.py:396
  19.3 7.6 %all-to-all-done.pieces_ref = f32[8,24,128]{2,1,0:T(8,128)S(1)} async-done(((f32[8,24,128]{2,1,0:T(8,128)}), f32[8,24,128]{2,1,0:T(8,128)S(1)}, u32[]{:S(2)}, u32[]{:S(2)}) %all-to-all-start) | async-done | bytes 98336 | tf_op jit(solution)/shard_map/all_to_all | solution.py:396
  26.9 0.1 along.1
  26.9 17.3 %all_to_all.30.pieces_ref = f32[8,16,128]{2,1,0:T(8,128)S(1)} all-to-all(f32[8,16,128]{2,1,0:T(8,128)S(1)} %get-tuple-element.12), channel_id=1, replica_groups=mesh['sp_0'=8,'sp_1'=8,'x'=4,'core'=2] {'sp_0'}, dimensions={0} | all-to-all | bytes 131072 | tf_op jit(solution)/shard_map/all_to_all | solution.py:396
  44.3 0.1 across.1
  44.4 10.4 %all_to_all.31.pieces_ref = f32[8,24,128]{2,1,0:T(8,128)S(1)} all-to-all(f32[8,24,128]{2,1,0:T(8,128)S(1)} %across.1), channel_id=1, replica_groups=mesh['sp_0'=8,'sp_1'=8,'x'=4,'core'=2] {'sp_1'}, dimensions={0} | all-to-all | bytes 196608 | tf_op jit(solution)/shard_map/all_to_all | solution.py:396
  54.8 3.9 %mix.1 = bf16[256,2048]{1,0:T(8,128)(2,1)S(1)} custom-call(f32[8,24,128]{2,1,0:T(8,128)S(1)} %all_to_all.31.pieces_ref, bf16[256,128]{1,0:T(8,128)(2,1)} %query_ref.1, bf16[256,128]{1,0:T(8,128)(2,1)} %key_ref.3, bf16[256,128]{1,0:T(8,128)(2,1)} %value_ref.3, f32[2,2,256]{2,1,0:T(2,128)} %rate_ref.3, f32[2,2,256]{2,1,0:T(2,128)} %fusion.2.decay_ref, ...), custom_call_target="tpu_custom_call" | custom-call | tf_op jit(solution)/shard_map/mix/pallas_call | solution.py:380
  58.8 23.3 %all_to_all.32.pieces_ref = bf16[8,32,2048]{2,1,0:T(8,128)(2,1)S(1)} all-to-all(bf16[8,32,2048]{2,1,0:T(8,128)(2,1)S(1)} %bitcast.29), channel_id=1, replica_groups=mesh['sp_0'=8,'sp_1'=8,'x'=4,'core'=2] {'x','core'}, dimensions={0} | all-to-all | bytes 2097152 | tf_op jit(solution)/shard_map/all_to_all | solution.py:396
  82.1 1.7 %norm.1 = (bf16[32,2048]{1,0:T(8,128)(2,1)}, bf16[8,32,2048]{2,1,0:T(8,128)(2,1)S(1)}) custom-call(bf16[8,32,2048]{2,1,0:T(8,128)(2,1)S(1)} %all_to_all.32.pieces_ref, bf16[32,2048]{1,0:T(8,128)(2,1)} %skip_ref.1, f32[1,2048]{1,0:T(1,128)} %bitcast.31), custom_call_target="tpu_custom_call" | custom-call | tf_op jit(solution)/shard_map/norm/pallas_call | solution.py:380
  83.8 18.4 %all_to_all.33 = bf16[8,32,2048]{2,1,0:T(8,128)(2,1)S(1)} all-to-all(bf16[8,32,2048]{2,1,0:T(8,128)(2,1)S(1)} %get-tuple-element.15), channel_id=1, replica_groups=mesh['sp_0'=8,'sp_1'=8,'x'=4,'core'=2] {'x','core'}, dimensions={0} | all-to-all | bytes 2097152 | tf_op jit(solution)/shard_map/all_to_all | solution.py:396
  102.2 0.0 copy-start
  102.2 1.4 collective-permute-start
  103.6 4.0 %collective-permute-start.1 = (bf16[1,2048]{1,0:T(2,128)(2,1)S(1)}, bf16[1,2048]{1,0:T(2,128)(2,1)S(1)}, u32[]{:S(2)}, u32[]{:S(2)}) collective-permute-start(bf16[1,2048]{1,0:T(2,128)(2,1)S(1)} %get-tuple-element.20), channel_id=1, source_target_pairs={{0,8},{8,16},{16,24},{24,32},{32,40},{40,48},{48,56},{56,64},{64,7... | collective-permute-start | bytes 12296 | tf_op jit(solution)/shard_map/ppermute | solution.py:466
  107.6 0.1 pad.7.clone
  107.7 0.7 pad.4.taps_ref
  108.4 0.0 collective-permute-done
  108.4 0.0 collective-permute-done.1
  108.4 0.1 maximum_maximum_fusion.edges_ref
  108.5 9.7 %all-gather.2.cloned.1.call-done.weight_ref = bf16[2048,2176]{1,0:T(8,128)(2,1)} async-done(((bf16[32,2176]{1,0:T(8,128)(2,1)}), bf16[2048,2176]{1,0:T(8,128)(2,1)}) %all-gather.2.cloned.1.call-update) | async-done | bytes 8912912 | tf_op jit(solution)/shard_map/all_gather | solution.py:422
  118.2 5.2 %feed.1 = (bf16[4,32,2048]{2,1,0:T(8,128)(2,1)S(1)}, bf16[256,768]{1,0:T(8,128)(2,1)S(1)}, bf16[2048,768]{1,0:T(8,128)(2,1)S(1)}) custom-call(s32[1]{0:T(128)} %bitcast.4.core_ref, bf16[256,2048]{1,0:T(8,128)(2,1)S(1)} %bitcast.28, bf16[16,2048]{1,0:T(8,128)(2,1)S(1)} %maximum_maximum_fusion.edges_ref, ...), custom_call_target="tpu_custom_call" | custom-call | tf_op jit(solution)/shard_map/feed/pallas_call | solution.py:471
  123.4 2.8 %collective-permute-start.2 = (bf16[4,32,2048]{2,1,0:T(8,128)(2,1)S(1)}, bf16[4,32,2048]{2,1,0:T(8,128)(2,1)S(1)}, u32[]{:S(2)}, u32[]{:S(2)}) collective-permute-start(bf16[4,32,2048]{2,1,0:T(8,128)(2,1)S(1)} %get-tuple-element.18), channel_id=1, source_target_pairs={{0,1},{1,0},{2,3},{3,2},{4,5},{5,4},{6,7},{7,6},{8,9},{9,8},{10,11... | collective-permute-start | bytes 1572872 | tf_op jit(solution)/shard_map/ppermute | solution.py:494
  126.2 1.1 own.1
  127.3 0.4 collective-permute-done.2
  127.7 0.1 add_convert_fusion
  127.8 12.4 %all_to_all.34 = bf16[4,32,2048]{2,1,0:T(8,128)(2,1)S(1)} all-to-all(bf16[4,32,2048]{2,1,0:T(8,128)(2,1)S(1)} %add_convert_fusion), channel_id=1, replica_groups=mesh['sp_0'=8,'sp_1'=8,'x'=4,'core'=2] {'x'}, dimensions={0} | all-to-all | bytes 1048576 | tf_op jit(solution)/shard_map/all_to_all | solution.py:396
  140.2 0.0 copy-done
  140.2 0.7 fusion
  (2 shorter events, 0.0 us)
Async XLA Ops:
  6.5 111.7 %all-gather.2.cloned.1.call-start = ((), (), s32[]{:S(2)}) async-start(), calls=%async_computation.6 | async-start | bytes 9052160 | tf_op jit(solution)/shard_map/all_gather | solution.py:422
  11.7 15.2 %all-to-all-start = ((f32[8,24,128]{2,1,0:T(8,128)}), f32[8,24,128]{2,1,0:T(8,128)S(1)}, u32[]{:S(2)}, u32[]{:S(2)}) async-start(f32[8,24,128]{2,1,0:T(8,128)} %summarize.1), calls=%async_computation | async-start | bytes 196608 | tf_op jit(solution)/shard_map/all_to_all | solution.py:396
  102.2 38.0 %copy-start = (bf16[32,2048]{1,0:T(8,128)(2,1)S(1)}, bf16[32,2048]{1,0:T(8,128)(2,1)}, u32[]{:S(2)}) copy-start(bf16[32,2048]{1,0:T(8,128)(2,1)} %get-tuple-element.14) | copy-start | bytes 393220
  102.2 6.2 %collective-permute-start = (bf16[1,2048]{1,0:T(2,128)(2,1)S(1)}, bf16[1,2048]{1,0:T(2,128)(2,1)S(1)}, u32[]{:S(2)}, u32[]{:S(2)}) collective-permute-start(bf16[1,2048]{1,0:T(2,128)(2,1)S(1)} %get-tuple-element.19), channel_id=1, source_target_pairs={{8,0},{16,8},{24,16},{32,24},{40,32},{48,40},{56,48},{64,56},{72,6... | collective-permute-start | bytes 12296 | tf_op jit(solution)/shard_map/ppermute | solution.py:467
  103.6 4.8 %collective-permute-start.1 = (bf16[1,2048]{1,0:T(2,128)(2,1)S(1)}, bf16[1,2048]{1,0:T(2,128)(2,1)S(1)}, u32[]{:S(2)}, u32[]{:S(2)}) collective-permute-start(bf16[1,2048]{1,0:T(2,128)(2,1)S(1)} %get-tuple-element.20), channel_id=1, source_target_pairs={{0,8},{8,16},{16,24},{24,32},{32,40},{40,48},{48,56},{56,64},{64,7... | collective-permute-start | bytes 12296 | tf_op jit(solution)/shard_map/ppermute | solution.py:466
  123.4 4.3 %collective-permute-start.2 = (bf16[4,32,2048]{2,1,0:T(8,128)(2,1)S(1)}, bf16[4,32,2048]{2,1,0:T(8,128)(2,1)S(1)}, u32[]{:S(2)}, u32[]{:S(2)}) collective-permute-start(bf16[4,32,2048]{2,1,0:T(8,128)(2,1)S(1)} %get-tuple-element.18), channel_id=1, source_target_pairs={{0,1},{1,0},{2,3},{3,2},{4,5},{5,4},{6,7},{7,6},{8,9},{9,8},{10,11... | collective-permute-start | bytes 1572872 | tf_op jit(solution)/shard_map/ppermute | solution.py:494
Sparse Core Ops, SparseCore 0:
  10.3 107.8 all-gather.1
